TPU v7x, 256 devices: a 2x2x32 block of a 4x8x32 slice. The times are simulated.
256 devices in a mesh: grp: 4 (over y, x), ep: 64 (over z, core).
Axes of the slice: x: 2, y: 2, z: 32, core: 2. Of those that a mesh axis runs over, the one named last changes fastest.
The devices are a block of a 4x8x32 slice.
Arguments:
- stream: bfloat16 [256, 2048], P('grp', 'ep'), parts along dimension 0, may hold values from -48 to 48
- conv_cache: bfloat16 [256, 3, 2560], P(('grp', 'ep')), parts along dimension 0, may hold values from -6 to 6
- scan_state: float32 [256, 32, 64, 128], P(('grp', 'ep')), parts along dimension 0, may hold values from -4 to 4
- gate_weight: bfloat16 [2048, 2048], P('ep'), may hold values from -0.125 to 0.125
- value_weight: bfloat16 [2048, 2048], P('ep'), may hold values from -0.125 to 0.125
- entry_weight: bfloat16 [2048, 256], P('ep'), may hold values from -0.125 to 0.125
- readout_weight: bfloat16 [2048, 256], P('ep'), may hold values from -0.125 to 0.125
- step_weight: bfloat16 [2048, 32], P('ep'), may hold values from -0.125 to 0.125
- conv_weight: bfloat16 [4, 2560], replicated, may hold values from -3 to 3
- step_bias: float32 [32], replicated, may hold values from -4 to -1
- decay_rate: float32 [32], replicated, may hold values from 0.5 to 8
- skip_gain: float32 [32], replicated, may hold values from 0.1 to 1.9
- group_gain: float32 [2048], replicated, may hold values from 0.1 to 1.9
- out_weight: bfloat16 [2048, 2048], P(None, 'ep'), may hold values from -0.125 to 0.125
- first_gain: float32 [2048], replicated, may hold values from 0.1 to 1.9
- routes: int32 [256, 4], P('grp'), parts along dimension 0, may hold values from 0 to 63, all different within a row; in each aligned block of 64 rows (0 to 63, 64 to 127, ...) at most 8 rows name the same one
- route_weight: float32 [256, 4], P('grp'), parts along dimension 0, may hold values from 0.1 to 1
- expert_gate: bfloat16 [64, 2048, 256], P('ep'), may hold values from -0.125 to 0.125
- expert_up: bfloat16 [64, 2048, 256], P('ep'), may hold values from -0.125 to 0.125
- expert_down: bfloat16 [64, 256, 2048], P('ep'), may hold values from -0.375 to 0.375
- shared_gate: bfloat16 [2048, 256], replicated, may hold values from -0.125 to 0.125
- shared_up: bfloat16 [2048, 256], replicated, may hold values from -0.125 to 0.125
- shared_down: bfloat16 [256, 2048], replicated, may hold values from -0.375 to 0.375
- second_gain: float32 [2048], P('ep'), may hold values from 0.1 to 1.9
Outputs:
- result: bfloat16 [256, 2048], P('grp', 'ep'), parts along dimension 0
- new_conv: bfloat16 [256, 3, 2560], P(('grp', 'ep')), parts along dimension 0
- new_state: float32 [256, 32, 64, 128], P(('grp', 'ep')), parts along dimension 0
There are 4 independent parts, one for each index of `grp`. A program takes and returns all parts, laid end to end along the dimension named above; an argument that names none is the same for every part. Nothing has to cross between parts.
Inputs may be any that keep to these rules, and one draw needn't show every extreme that they name: `routes`: each row names 4 different experts; no expert is named by more than 8 rows, a bound that some block reaches.
All inputs are finite; a program needn't handle non-finite values.
Results may differ from a plain program's by a relative error of at most 0.0065.
Values may be sent and summed in bfloat16 or wider, within the bound.
A program may use at most 64 MiB of HBM per device.

v0:
```python
import jax
import jax.numpy as jnp
from jax import lax
from jax.sharding import PartitionSpec as P

HEAD_DIM = 64
STATE = 128
GROUPS = 2
CAP = 8


RESIDUAL_SCALE = 2.0**0.25
NORM_EPSILON = 1e-05
GATED_EPSILON = 1e-06


def in_blocks(x, dim, length):
    lengths = x.shape
    tiles = x.reshape(*lengths[:dim], length, lengths[dim] // length, *lengths[dim + 1 :])
    return jnp.moveaxis(tiles, dim, 0)


def sent_and_summed(x, axis, dim):
    tiles = in_blocks(x, dim, lax.axis_size(axis))
    arrived = lax.all_to_all(tiles, axis, split_axis=0, concat_axis=0, tiled=True)
    return arrived.sum(axis=0)


def from_everyone(x, axis):
    copies = jnp.broadcast_to(x, (lax.axis_size(axis), *x.shape))
    return lax.all_to_all(copies, axis, split_axis=0, concat_axis=0, tiled=True)


def in_order(tiles, dim):
    lengths = list(tiles.shape[1:])
    lengths[dim] *= tiles.shape[0]
    return jnp.moveaxis(tiles, 0, dim).reshape(lengths)


def gather_directly(x, axis, dim):
    tiles = from_everyone(x, axis)
    return in_order(tiles, dim)


def turned_gather(arrays, axis, dims):
    turned = [jnp.moveaxis(a, dim, 0) for a, dim in zip(arrays, dims)]
    both = jnp.concatenate([t.reshape(len(t), -1) for t in turned], axis=1)
    result, at, finished = (lax.all_gather(both, axis, axis=0, tiled=True), 0, [])
    for t, dim in zip(turned, dims):
        slab = result[:, at : at + t[0].size].reshape(-1, *t.shape[1:])
        finished.append(jnp.moveaxis(slab, 0, dim))
        at += t[0].size
    return tuple(finished)


def over_copies(x, axis):
    everything = from_everyone(x, axis)
    return jnp.sum(everything, axis=0)


def in_one(arrays, axis):
    line, at, finished = (jnp.concatenate([a.reshape(-1) for a in arrays]), 0, [])
    total = over_copies(line, axis)
    for a in arrays:
        finished.append(total[at : at + a.size].reshape(a.shape))
        at += a.size
    return tuple(finished)


def rounded(value):
    return lax.optimization_barrier(value.astype(jnp.bfloat16))


def finish_norm(residual, row_total, square, full_width, gain):
    mean_value = (row_total / full_width)[:, None]
    variance = (square / full_width)[:, None] - mean_value * mean_value
    return (residual - mean_value) * lax.rsqrt(variance + NORM_EPSILON) * gain


def swiglu(inputs, gate_matrix, up_matrix, down_matrix):
    hidden = (
        jax.nn.silu(jnp.dot(inputs, gate_matrix, preferred_element_type=jnp.float32))
        * jnp.dot(inputs, up_matrix, preferred_element_type=jnp.float32)
    ).astype(jnp.bfloat16)
    return rounded(jnp.dot(hidden, down_matrix, preferred_element_type=jnp.float32))


def on_device(
    stream,
    conv_cache,
    scan_state,
    gate_weight,
    value_weight,
    entry_weight,
    readout_weight,
    step_weight,
    conv_weight,
    step_bias,
    decay_rate,
    skip_gain,
    group_gain,
    out_weight,
    first_gain,
    routes,
    route_weight,
    expert_gate,
    expert_up,
    expert_down,
    shared_gate,
    shared_up,
    shared_down,
    second_gain,
):
    devices = lax.axis_size("ep")
    device_rank = lax.axis_index("ep")
    own_rows = conv_cache.shape[0]
    row_count = stream.shape[0]
    slice_width = stream.shape[1]
    full_width = slice_width * devices
    inner_width = gate_weight.shape[1]
    head_count = step_weight.shape[1]
    per_group = head_count // GROUPS
    group_width = inner_width // GROUPS
    bounds = (inner_width, 2 * inner_width + 2 * GROUPS * STATE)
    weights_in = (gate_weight, value_weight, entry_weight, readout_weight, step_weight)
    summed = rounded(
        sent_and_summed(
            jnp.concatenate(
                [
                    jnp.dot(stream, weight, preferred_element_type=jnp.float32)
                    for weight in weights_in
                ],
                axis=1,
            ),
            "ep",
            0,
        )
    )
    gate_rows = summed[:, : bounds[0]]
    fresh = summed[:, bounds[0] : bounds[1]]
    step_rows = summed[:, bounds[1] :]
    window = jnp.concatenate([conv_cache, fresh[:, None, :]], axis=1)
    active = jax.nn.silu(
        jnp.sum(window.astype(jnp.float32) * conv_weight.astype(jnp.float32)[None], axis=1)
    )
    head_in = active[:, :inner_width].reshape(own_rows, GROUPS, per_group, HEAD_DIM)
    entry_rows = active[:, inner_width : inner_width + GROUPS * STATE].reshape(
        own_rows, GROUPS, 1, 1, STATE
    )
    readout_rows = active[:, inner_width + GROUPS * STATE :].reshape(own_rows, GROUPS, 1, 1, STATE)
    step_size = jax.nn.softplus(step_rows.astype(jnp.float32) + step_bias).reshape(
        own_rows, GROUPS, per_group
    )
    retained = jnp.exp(-step_size * decay_rate.reshape(GROUPS, per_group))
    old_state = scan_state.reshape(own_rows, GROUPS, per_group, HEAD_DIM, STATE)
    new_state = (
        retained[..., None, None] * old_state
        + (step_size[..., None] * head_in)[..., None] * entry_rows
    )
    head_out = (
        jnp.sum(new_state * readout_rows, axis=-1)
        + skip_gain.reshape(GROUPS, per_group)[:, :, None] * head_in
    )
    gated_out = head_out.reshape(own_rows, GROUPS, group_width) * jax.nn.silu(
        gate_rows.astype(jnp.float32)
    ).reshape(own_rows, GROUPS, group_width)
    normed = gated_out * lax.rsqrt(
        jnp.mean(gated_out * gated_out, axis=-1, keepdims=True) + GATED_EPSILON
    )
    normed = (normed.reshape(own_rows, inner_width) * group_gain).astype(jnp.bfloat16)
    mixer_out = rounded(
        jnp.dot(gather_directly(normed, "ep", 0), out_weight, preferred_element_type=jnp.float32)
    )
    column_start = device_rank * slice_width
    whole_stream, whole_mixer = turned_gather((stream, mixer_out), "ep", (1, 1))
    residual = RESIDUAL_SCALE * whole_stream.astype(jnp.float32) + whole_mixer.astype(jnp.float32)
    first_rows = rounded(
        finish_norm(
            residual,
            jnp.sum(residual, axis=1),
            jnp.sum(residual * residual, axis=1),
            full_width,
            first_gain,
        )
    )
    first_part = lax.dynamic_slice_in_dim(first_rows, column_start, slice_width, 1)
    matches = routes[:, :, None] == jnp.arange(devices, dtype=jnp.int32)[None, None, :]
    member = jnp.sum(matches.astype(jnp.int32), axis=1)
    weight_of = jnp.sum(jnp.where(matches, route_weight[:, :, None], 0.0), axis=1)
    slot_rank = jnp.cumsum(member, axis=0) - member
    slot_ids = jnp.arange(CAP, dtype=jnp.int32)
    mine_member = lax.dynamic_slice_in_dim(member, device_rank, 1, 1)[:, 0]
    mine_slot = lax.dynamic_slice_in_dim(slot_rank, device_rank, 1, 1)[:, 0]
    chosen = (mine_slot[None, :] == slot_ids[:, None]) & (mine_member[None, :] == 1)
    taken_rows = jnp.dot(
        chosen.astype(jnp.bfloat16), first_rows, preferred_element_type=jnp.float32
    ).astype(jnp.bfloat16)
    expert_out = swiglu(taken_rows, expert_gate[0], expert_up[0], expert_down[0])
    arrived = lax.all_to_all(expert_out, "ep", split_axis=1, concat_axis=0, tiled=True)
    spread = jnp.where(
        (slot_rank[:, :, None] == slot_ids[None, None, :]) & (member[:, :, None] == 1),
        weight_of[:, :, None],
        0.0,
    )
    moe_part = jnp.dot(spread.reshape(row_count, devices * CAP), arrived.astype(jnp.float32))
    down_part = lax.dynamic_slice_in_dim(shared_down, column_start, slice_width, 1)
    shared_part = swiglu(first_rows, shared_gate, shared_up, down_part)
    moe_part = moe_part + shared_part.astype(jnp.float32)
    residual_two = RESIDUAL_SCALE * first_part.astype(jnp.float32) + moe_part
    total_two, square_two = in_one(
        (jnp.sum(residual_two, axis=1), jnp.sum(residual_two * residual_two, axis=1)), "ep"
    )
    result = finish_norm(residual_two, total_two, square_two, full_width, second_gain).astype(
        jnp.bfloat16
    )
    return (result, window[:, 1:], new_state.reshape(own_rows, head_count, HEAD_DIM, STATE))


def solution(mesh):
    return jax.shard_map(
        on_device,
        mesh=mesh,
        in_specs=(
            P("grp", "ep"),
            P(("grp", "ep"), None, None),
            P(("grp", "ep"), None, None, None),
            P("ep", None),
            P("ep", None),
            P("ep", None),
            P("ep", None),
            P("ep", None),
            P(),
            P(),
            P(),
            P(),
            P(),
            P(None, "ep"),
            P(),
            P("grp", None),
            P("grp", None),
            P("ep", None, None),
            P("ep", None, None),
            P("ep", None, None),
            P(),
            P(),
            P(),
            P("ep"),
        ),
        out_specs=(
            P("grp", "ep"),
            P(("grp", "ep"), None, None),
            P(("grp", "ep"), None, None, None),
        ),
        check_vma=False,
    )
```

profile of v0, /device:TPU:37, one launch (start us, length us, event | category | flops | bytes accessed | tf_op | source)
XLA Modules:
  0.0 340.1 jit_solution(15785676046890249651)
XLA Ops:
  0.7 1.2 convolution_dynamic-update-slice_fusion.1
  1.9 1.2 convolution_dynamic-update-slice_fusion
  3.1 0.2 convolution_dynamic-update-slice_fusion.3
  3.3 0.2 convolution_dynamic-update-slice_fusion.2
  3.5 0.2 convolution_dynamic-update-slice_fusion.4
  3.7 2.3 copy.46
  5.9 34.5 %all-to-all-start = ((f32[64,1,4640]{2,1,0:T(1,128)}), f32[64,1,4640]{2,1,0:T(1,128)S(1)}, u32[]{:S(2)}, u32[]{:S(2)}) async-start(f32[64,1,4640]{2,1,0:T(1,128)} %copy.46), calls=%async_computation | async-start | bytes 2424832 | tf_op jit(solution)/shard_map/all_to_all | solution.py:25
  40.8 123.8 %all-to-all-done = f32[64,1,4640]{2,1,0:T(1,128)S(1)} async-done(((f32[64,1,4640]{2,1,0:T(1,128)}), f32[64,1,4640]{2,1,0:T(1,128)S(1)}, u32[]{:S(2)}, u32[]{:S(2)}) %all-to-all-start) | async-done | bytes 1187872 | tf_op jit(solution)/shard_map/all_to_all | solution.py:25
  164.6 1.0 reduce_sum.105
  166.0 1.4 multiply_reduce_fusion.1
  167.5 0.5 broadcast.179
  168.0 0.7 fusion.49
  168.7 0.1 multiply_reduce_fusion.4
  169.0 0.3 broadcast_in_dim.29
  169.3 0.5 broadcast.180
  169.8 2.2 reduce.24
  172.0 0.9 reshape.316
  172.9 5.3 %all-to-all-start.1 = ((bf16[64,2,1024]{2,1,0:T(2,128)(2,1)}), bf16[64,2,1024]{2,1,0:T(2,128)(2,1)S(1)}, u32[]{:S(2)}, u32[]{:S(2)}) async-start(bf16[64,2,1024]{2,1,0:T(2,128)(2,1)} %reshape.316), calls=%async_computation.1 | async-start | bytes 524288 | tf_op jit(solution)/shard_map/all_to_all | solution.py:31
  178.2 0.1 convert_reduce_fusion
  178.3 0.1 reduce_window_sum.11
  178.4 0.2 dynamic-slice_reduce_fusion
  178.6 0.2 fusion.30
  178.8 0.1 select_reduce_fusion
  178.9 41.9 %all-to-all-done.1 = bf16[64,2,1024]{2,1,0:T(2,128)(2,1)S(1)} async-done(((bf16[64,2,1024]{2,1,0:T(2,128)(2,1)}), bf16[64,2,1024]{2,1,0:T(2,128)(2,1)S(1)}, u32[]{:S(2)}, u32[]{:S(2)}) %all-to-all-start.1) | async-done | bytes 262176 | tf_op jit(solution)/shard_map/all_to_all | solution.py:31
  220.8 0.2 reshape.317
  221.1 0.3 convolution_convert_fusion.2
  221.4 54.9 %all_gather.3 = bf16[2048,128]{1,0:T(8,128)(2,1)S(1)} all-gather(bf16[32,128]{1,0:T(8,128)(2,1)S(1)} %pad_maximum_fusion.1), channel_id=1, replica_groups=mesh['grp'=4,'ep'=64] {'ep'}, dimensions={0}, use_global_device_ids=true | all-gather | bytes 532480 | tf_op jit(solution)/shard_map/all_gather | solution.py:48
  276.4 0.4 fusion.11
  276.8 0.5 fusion.12
  277.3 0.2 convolution_convert_fusion.1
  277.5 0.5 copy-done.3
  278.0 0.2 fusion.9
  278.2 0.3 copy-done.4
  278.5 0.7 convolution_convert_fusion
  279.2 0.2 all_to_all.24
  279.5 0.7 reshape.318
  280.2 7.1 %all-to-all-start.2 = ((bf16[64,2,128]{2,1,0:T(2,128)(2,1)}), bf16[64,2,128]{2,1,0:T(2,128)(2,1)S(1)}, u32[]{:S(2)}, u32[]{:S(2)}) async-start(bf16[64,2,128]{2,1,0:T(2,128)(2,1)} %reshape.318), calls=%async_computation.2 | async-start | bytes 65536 | tf_op jit(solution)/shard_map/all_to_all | solution.py:199
  287.3 1.5 fusion.52
  288.9 1.3 fusion.4
  290.2 19.6 %all-to-all-done.2 = bf16[64,2,128]{2,1,0:T(2,128)(2,1)S(1)} async-done(((bf16[64,2,128]{2,1,0:T(2,128)(2,1)}), bf16[64,2,128]{2,1,0:T(2,128)(2,1)S(1)}, u32[]{:S(2)}, u32[]{:S(2)}) %all-to-all-start.2) | async-done | bytes 32800 | tf_op jit(solution)/shard_map/all_to_all | solution.py:199
  309.8 0.1 reshape.319
  309.9 0.1 copy.48
  310.1 0.2 fusion.47
  310.3 0.6 broadcast_in_dim.38
  311.0 5.6 %all-to-all-start.3 = ((f32[64,1,128]{2,1,0:T(1,128)}), f32[64,1,128]{2,1,0:T(1,128)S(1)}, u32[]{:S(2)}, u32[]{:S(2)}) async-start(f32[64,1,128]{2,1,0:T(1,128)} %broadcast_in_dim.38), calls=%async_computation.3 | async-start | bytes 65536 | tf_op jit(solution)/shard_map/all_to_all | solution.py:31
  316.6 0.6 pad_maximum_fusion
  317.2 22.1 %all-to-all-done.3 = f32[64,1,128]{2,1,0:T(1,128)S(1)} async-done(((f32[64,1,128]{2,1,0:T(1,128)}), f32[64,1,128]{2,1,0:T(1,128)S(1)}, u32[]{:S(2)}, u32[]{:S(2)}) %all-to-all-start.3) | async-done | bytes 32800 | tf_op jit(solution)/shard_map/all_to_all | solution.py:31
  339.5 0.7 multiply_convert_fusion.1
  (68 shorter events, 1.4 us)
Async XLA Ops:
  0.6 277.6 %copy-start = (bf16[1,256,2048]{2,1,0:T(8,128)(2,1)S(1)}, bf16[1,256,2048]{2,1,0:T(8,128)(2,1)}, u32[]{:S(2)}) copy-start(bf16[1,256,2048]{2,1,0:T(8,128)(2,1)} %param.43) | copy-start | bytes 3145732
  0.6 2.5 copy-start.5
  0.7 2.5 copy-start.8
  0.7 2.6 copy-start.9
  0.7 2.8 copy-start.12
  5.9 34.5 %copy-start.19 = (f32[32]{0:T(128)S(1)}, f32[32]{0:T(128)}, u32[]{:S(2)}) copy-start(f32[32]{0:T(128)} %param.35) | copy-start | bytes 388
  5.9 158.6 %all-to-all-start = ((f32[64,1,4640]{2,1,0:T(1,128)}), f32[64,1,4640]{2,1,0:T(1,128)S(1)}, u32[]{:S(2)}, u32[]{:S(2)}) async-start(f32[64,1,4640]{2,1,0:T(1,128)} %copy.46), calls=%async_computation | async-start | bytes 2424832 | tf_op jit(solution)/shard_map/all_to_all | solution.py:25
  40.4 125.2 %copy-start.6 = (bf16[1,3,2560]{2,1,0:T(4,128)(2,1)S(1)}, bf16[1,3,2560]{2,1,0:T(4,128)(2,1)}, u32[]{:S(2)}) copy-start(bf16[1,3,2560]{2,1,0:T(4,128)(2,1)} %param.25) | copy-start | bytes 46084
  40.4 125.2 %copy-start.7 = (bf16[4,2560]{1,0:T(4,128)(2,1)S(1)}, bf16[4,2560]{1,0:T(4,128)(2,1)}, u32[]{:S(2)}) copy-start(bf16[4,2560]{1,0:T(4,128)(2,1)} %param.32) | copy-start | bytes 61444
  40.4 125.4 %copy-start.15 = (f32[32]{0:T(128)S(1)}, f32[32]{0:T(128)}, u32[]{:S(2)}) copy-start(f32[32]{0:T(128)} %param.34) | copy-start | bytes 388
  40.4 125.4 %copy-start.16 = (f32[32]{0:T(128)S(1)}, f32[32]{0:T(128)}, u32[]{:S(2)}) copy-start(f32[32]{0:T(128)} %param.33) | copy-start | bytes 388
  40.5 125.5 %copy-start.1 = (f32[1,32,64,128]{3,2,1,0:T(8,128)S(1)}, f32[1,32,64,128]{3,2,1,0:T(8,128)}, u32[]{:S(2)}) copy-start(f32[1,32,64,128]{3,2,1,0:T(8,128)} %param.26) | copy-start | bytes 3145732
  165.9 3.1 copy-start.13
  169.0 9.2 %copy-start.11 = (s32[64,4]{0,1:T(4,128)S(1)}, s32[64,4]{0,1:T(4,128)}, u32[]{:S(2)}) copy-start(s32[64,4]{0,1:T(4,128)} %param.39) | copy-start | bytes 3076
  169.0 9.8 %copy-start.14 = (f32[64,4]{0,1:T(4,128)S(1)}, f32[64,4]{0,1:T(4,128)}, u32[]{:S(2)}) copy-start(f32[64,4]{0,1:T(4,128)} %param.40) | copy-start | bytes 3076
  172.0 49.0 %copy-start.18 = (bf16[2048,32]{0,1:T(8,128)(2,1)S(1)}, bf16[2048,32]{0,1:T(8,128)(2,1)}, u32[]{:S(2)}) copy-start(bf16[2048,32]{0,1:T(8,128)(2,1)} %param.37) | copy-start | bytes 393220
  172.9 47.9 %all-to-all-start.1 = ((bf16[64,2,1024]{2,1,0:T(2,128)(2,1)}), bf16[64,2,1024]{2,1,0:T(2,128)(2,1)S(1)}, u32[]{:S(2)}, u32[]{:S(2)}) async-start(bf16[64,2,1024]{2,1,0:T(2,128)(2,1)} %reshape.316), calls=%async_computation.1 | async-start | bytes 524288 | tf_op jit(solution)/shard_map/all_to_all | solution.py:31
  221.0 55.7 %copy-start.10 = (f32[2048]{0:T(1024)S(1)}, f32[2048]{0:T(1024)}, u32[]{:S(2)}) copy-start(f32[2048]{0:T(1024)} %param.38) | copy-start | bytes 24580
  276.7 1.2 copy-start.3
  277.3 1.2 copy-start.4
  279.2 9.7 %copy-start.2 = (bf16[2048,256]{1,0:T(8,128)(2,1)S(1)}, bf16[2048,256]{1,0:T(8,128)(2,1)}, u32[]{:S(2)}) copy-start(bf16[2048,256]{1,0:T(8,128)(2,1)} %param.45) | copy-start | bytes 3145732
  280.2 29.6 %all-to-all-start.2 = ((bf16[64,2,128]{2,1,0:T(2,128)(2,1)}), bf16[64,2,128]{2,1,0:T(2,128)(2,1)S(1)}, u32[]{:S(2)}, u32[]{:S(2)}) async-start(bf16[64,2,128]{2,1,0:T(2,128)(2,1)} %reshape.318), calls=%async_computation.2 | async-start | bytes 65536 | tf_op jit(solution)/shard_map/all_to_all | solution.py:199
  288.9 50.6 %copy-start.17 = (f32[32]{0:T(128)S(1)}, f32[32]{0:T(128)}, u32[]{:S(2)}) copy-start(f32[32]{0:T(128)} %param.47) | copy-start | bytes 388
  311.0 28.4 %all-to-all-start.3 = ((f32[64,1,128]{2,1,0:T(1,128)}), f32[64,1,128]{2,1,0:T(1,128)S(1)}, u32[]{:S(2)}, u32[]{:S(2)}) async-start(f32[64,1,128]{2,1,0:T(1,128)} %broadcast_in_dim.38), calls=%async_computation.3 | async-start | bytes 65536 | tf_op jit(solution)/shard_map/all_to_all | solution.py:31
where the time goes:
time: 341 us; the launch traced here: 340 us
  waiting for transfers between devices  207 us (61%)
  blocking collectives  54.9 us (16%)
  starting transfers between devices  52.5 us (15%)
  other arithmetic  8.58 us (3%)
  local copies, waits for them, and re-layouts  8.24 us (2%)
  matrix products  7.42 us (2%)
    all_to_all x1, waiting for transfers between devices, sent_and_summed(): lax.all_to_all(tiles, axis, split_axis=0, concat_axis=0, tiled=True)  124 us
    all_to_all x2, waiting for transfers between devices, from_everyone(): return lax.all_to_all(copies, axis, split_axis=0, concat_axis=0, tiled=True)  64 us
    all_gather x1, blocking collectives, turned_gather(): lax.all_gather(both, axis, axis=0, tiled=True)  54.9 us
    all_to_all x1, starting transfers between devices, sent_and_summed(): lax.all_to_all(tiles, axis, split_axis=0, concat_axis=0, tiled=True)  34.5 us
    all_to_all x1, waiting for transfers between devices, on_device(): lax.all_to_all(expert_out, 'ep', split_axis=1, concat_axis=0, tiled=True)  19.6 us
    all_to_all x2, starting transfers between devices, from_everyone(): return lax.all_to_all(copies, axis, split_axis=0, concat_axis=0, tiled=True)  10.9 us
    all_to_all x1, starting transfers between devices, on_device(): lax.all_to_all(expert_out, 'ep', split_axis=1, concat_axis=0, tiled=True)  7.1 us
  transfers between devices with their start and end apart: 4, of which 4 were waited for; matrix products, arithmetic and copies ran while one was open for 1% of the time, Pallas kernels for 0%

commit v1 on v0

v1 whole, which is shorter than its diff:
```python
import functools

import jax
import jax.numpy as jnp
from jax import lax
from jax.experimental import pallas as pl
from jax.experimental.pallas import tpu as pltpu
from jax.sharding import PartitionSpec as P

GROUPS = 2
CAP = 8
LANES = 128
WINDOW = 8
RESIDUAL_SCALE = 2.0**0.25
NORM_EPSILON = 1e-05
GATED_EPSILON = 1e-06
F32 = jnp.float32
BF16 = jnp.bfloat16
NT = (((1,), (1,)), ((), ()))


def mm(a, b):
    return jnp.dot(a, b, preferred_element_type=F32)


def mm_nt(a, b):
    return lax.dot_general(a, b, NT, preferred_element_type=F32)


def iota(shape, dim):
    return lax.broadcasted_iota(jnp.int32, shape, dim)


def silu(x):
    return x * jax.nn.sigmoid(x)


def one_hot(hit):
    return jnp.where(hit, 1.0, 0.0).astype(BF16)


def half_turn(x):
    return pltpu.roll(x, LANES // 2, x.ndim - 1)


def kernel(dims, *refs):
    chips, heads, vec_rows, main_rows, gate_rows = dims
    (
        stream, conv_cache, state_in, w_gate, w_value, w_entry, w_readout, w_step, conv_w, step_bias, decay, skip,
        group_gain, w_out, first_gain, routes, route_w, e_gate, e_up, e_down, s_gate, s_up, s_down, second_gain,
        o_result, o_conv, o_state,
        x_stream, x_cache, x_state, x_gate, x_value, x_entry, x_readout, x_step, x_conv_w, x_bias, x_decay, x_skip,
        x_ggain, x_out, x_fgain, x_routes, x_route_w, x_eg, x_eu, x_ed, x_sg, x_su, x_sd, x_sgain,
        conv_rows, tap_rows, base_rows, chosen_s, spread_s,
        q_main, sa_main, ra_main, qb_main, sb_main, rb_main, sc_main, rc_main,
        q_gate, sa_gate, ra_gate, qb_gate, sb_gate, rb_gate, sc_gate, rc_gate,
        fresh_row, n_rows, n_wide, r_rows, res_s, first_s, s_exp, r_exp, base_two, m_part, r_part, stat_s, final_s,
        local_sem, sib_sem, ssib_sem, round_sem, p_send, p_recv, x_send, x_recv, out_sem,
    ) = refs
    me = lax.axis_index("ep")
    z, c = me // 2, lax.rem(me, 2)
    p, h = lax.rem(z, 2), z // 2
    half = chips // 2
    quarter = half // 4
    pairs = half // 2

    def device(zz, cc):
        return {"ep": zz * 2 + cc}

    def wrap(value, n):
        return lax.rem(value + n, n)

    def send(src, dst, ssem, rsem, zz, cc):
        return pltpu.make_async_remote_copy(
            src, dst, ssem, rsem, device_id=device(zz, cc), device_id_type=pl.DeviceIdType.MESH
        )

    def arrived(ref, sem):
        pltpu.make_async_copy(ref, ref, sem).wait()

    def signal(sem, zz, cc):
        pl.semaphore_signal(sem, inc=1, device_id=device(zz, cc), device_id_type=pl.DeviceIdType.MESH)

    barrier = pltpu.get_barrier_semaphore()
    signal(barrier, z, 1 - c)
    signal(barrier, wrap(z + 1, chips), c)
    signal(barrier, wrap(z - 1, chips), c)

    shared_in = ((stream, x_stream), (w_value, x_value), (w_entry, x_entry), (w_readout, x_readout), (w_step, x_step),
                 (w_gate, x_gate), (w_out, x_out))
    loads = []
    for src, dst in shared_in:
        loads.append((src, dst.at[c]))
    for pair in (
        (conv_cache, x_cache), (conv_w, x_conv_w), (routes, x_routes), (route_w, x_route_w), (step_bias, x_bias),
        (decay, x_decay), (skip, x_skip), (group_gain, x_ggain), (first_gain, x_fgain), (second_gain, x_sgain),
        (state_in, x_state), (e_gate, x_eg), (e_up, x_eu), (e_down, x_ed), (s_gate, x_sg), (s_up, x_su),
    ):
        loads.append(pair)
    chunks_d = x_sd.shape[0]
    for k in range(chunks_d):
        loads.append((s_down.at[:, pl.ds(k * LANES, LANES)], x_sd.at[k]))
    loads = [pltpu.make_async_copy(s, d, local_sem.at[i]) for i, (s, d) in enumerate(loads)]
    for copy in loads:
        copy.start()

    pl.semaphore_wait(barrier, 3)
    swaps = [
        send(src, dst.at[c], ssib_sem.at[i], sib_sem.at[i], z, 1 - c) for i, (src, dst) in enumerate(shared_in)
    ]
    for copy in swaps:
        copy.start()

    def round_signal(i, d):
        signal(round_sem.at[i], wrap(z + d, chips), c)
        signal(round_sem.at[i], wrap(z - d, chips), c)

    def round_wait(i):
        pl.semaphore_wait(round_sem.at[i], 2)

    round_signal(0, 1)

    count = x_routes.shape[1]
    for i in (7, 8, 9, 10):
        loads[i].wait()
    expert_of = iota((2 * chips, count), 0)
    member, weight = jnp.zeros((2 * chips, count), F32), jnp.zeros((2 * chips, count), F32)
    for k in range(x_routes.shape[0]):
        hit = expert_of == x_routes[k : k + 1, :]
        member = member + jnp.where(hit, 1.0, 0.0)
        weight = weight + jnp.where(hit, x_route_w[k : k + 1, :], 0.0)
    row, col = iota((count, count), 0), iota((count, count), 1)
    order = one_hot(col == 2 * lax.rem(row, chips) + row // chips)
    w_hi = weight.astype(BF16)
    w_lo = (weight - w_hi.astype(F32)).astype(BF16)
    member = mm_nt(order, member.astype(BF16)).astype(BF16)
    w_hi = mm_nt(order, w_hi).astype(BF16)
    w_lo = mm_nt(order, w_lo).astype(BF16)
    rank = mm(one_hot(col < row), member).astype(BF16)
    mine = one_hot(iota((CAP, 2 * chips), 1) == me)
    mine_rank, mine_member = mm_nt(mine, rank), mm_nt(mine, member)
    slot = iota((CAP, count), 0).astype(F32)
    chosen_s[...] = one_hot((mine_member > 0.5) & (mine_rank == slot))
    wide = chips * CAP
    pick = one_hot(iota((2 * chips, wide), 0) == 2 * (iota((2 * chips, wide), 1) // CAP) + c)
    slot = lax.rem(iota((count, wide), 1), CAP).astype(F32)
    fits = (mm(member, pick) > 0.5) & (mm(rank, pick) == slot)
    spread_s[0:count, :] = jnp.where(fits, mm(w_hi, pick), 0.0).astype(BF16)
    spread_s[count : 2 * count, :] = jnp.where(fits, mm(w_lo, pick), 0.0).astype(BF16)

    taps = x_conv_w.shape[0]
    conv_chunks = x_conv_w.shape[1] // LANES
    cache = x_cache[0].astype(F32)
    tap = x_conv_w[...].astype(F32)
    tap_rows[...] = jnp.zeros_like(tap_rows)
    conv_rows[...] = jnp.zeros_like(conv_rows)
    for k in range(conv_chunks):
        tap_rows[pl.ds(k, taps, stride=main_rows), :] = tap[:, k * LANES : (k + 1) * LANES]
        conv_rows[pl.ds(k, taps - 1, stride=main_rows), :] = cache[:, k * LANES : (k + 1) * LANES]
    early = jnp.zeros((main_rows, LANES), F32)
    for j in range(taps - 1):
        at = slice(j * main_rows, (j + 1) * main_rows)
        early = early + conv_rows[at, :] * tap_rows[at, :]
    base_rows[...] = early

    round_wait(0)
    round_signal(1, 2)
    for i in range(5):
        loads[i].wait()
        swaps[i].wait_recv()
    both = x_stream[...].reshape(-1, count)
    row, col = iota((chips, count), 0), iota((chips, count), 1)
    within = lax.rem(row, half)
    chip_of = 2 * (within // 2 + pairs * lax.rem(within, 2)) + row // half
    lhs = mm_nt(one_hot(col == 2 * chip_of + c), both).astype(BF16)

    def two(ref):
        return ref[...].reshape(-1, ref.shape[-1])

    def fill(q, rows, first, product):
        for k in range(product.shape[1] // LANES):
            q[pl.ds(first + k, chips, stride=rows), :] = product[:, k * LANES : (k + 1) * LANES]

    zero = jnp.zeros((chips, LANES), F32)
    fill(q_main, main_rows, 0, mm(lhs, two(x_value)))
    fill(q_main, main_rows, vec_rows, mm(lhs, two(x_entry)))
    fill(q_main, main_rows, vec_rows + GROUPS, mm(lhs, two(x_readout)))
    steps = mm(lhs, two(x_step))
    steps = jnp.concatenate([steps, zero[:, : LANES - steps.shape[1]]], axis=1)
    fill(q_main, main_rows, vec_rows + 2 * GROUPS, steps)
    for k in range(vec_rows + 2 * GROUPS + 1, main_rows):
        fill(q_main, main_rows, k, zero)

    across = z + 1 - 2 * p
    step_at = (vec_rows + 2 * GROUPS) % 8

    def to_send(total, n, rows):
        blocks = total.reshape(n, rows // 8, 8, LANES)
        if rows == gate_rows:
            return blocks.astype(BF16)
        tail = blocks[:, -1]
        whole = tail[:, step_at : step_at + 1] + tail[:, step_at + 1 : step_at + 2]
        near = whole.astype(BF16).astype(F32)
        at = iota(tail.shape, 1)
        tail = jnp.where(at == step_at, near, jnp.where(at == step_at + 1, whole - near, tail))
        return jnp.concatenate([blocks[:, :-1], tail[:, None]], axis=1).astype(BF16)

    def stage_a(i, rows, q, sa, ra):
        start = pl.multiple_of((1 - p) * half * rows, half * rows)
        sa[...] = to_send(q[pl.ds(start, half * rows), :], half, rows)
        copy = send(sa, ra, p_send.at[i], p_recv.at[i], across, c)
        copy.start()
        return copy

    def stage_b(i, rows, q, ra, qb, sb, rb):
        start = pl.multiple_of(p * half * rows, half * rows)
        total = q[pl.ds(start, half * rows), :] + ra[...].astype(F32).reshape(half * rows, LANES)
        qb[...] = total
        sb[...] = to_send(total, half, rows).reshape(sb.shape)
        u, v = lax.rem(h, pairs), h // pairs
        target = 2 * wrap(h - quarter, half) + p
        last = rb.shape[0] - 1
        copies = [send(sb.at[u, 1 - v], rb.at[last], p_send.at[i], p_recv.at[i], target, c)]
        for n, e in enumerate(x for k in range(quarter - 1, 0, -1) for x in (k, -k)):
            u = lax.rem(h + e + quarter + half, pairs)
            target = 2 * wrap(h + e, half) + p
            copies.append(send(sb.at[u], rb.at[pl.ds(2 * n, 2)], p_send.at[i], p_recv.at[i], target, c))
        for copy in copies:
            copy.start()

    minus = wrap(h - quarter, half) // pairs

    def stage_c(i, rows, qb, rb, sc, rc):
        u = lax.rem(h + quarter, pairs)
        start = pl.multiple_of(u * 2 * rows, 2 * rows)
        total = qb[pl.ds(start, 2 * rows), :].reshape(2, rows, LANES)
        last = rb.shape[0] - 1
        for n in range(0, last, 2):
            total = total + rb[n : n + 2].astype(F32).reshape(2, rows, LANES)
        extra = rb[last].astype(F32).reshape(rows, LANES)
        for v in range(2):
            sc[v] = to_send(total[v] + jnp.where(minus == v, extra, 0.0), 1, rows)[0]
        for n, (v, target) in enumerate(((minus, h - quarter), (1 - minus, h + quarter))):
            send(sc.at[v], rc.at[n], p_send.at[i], p_recv.at[i], 2 * wrap(target, half) + p, c).start()

    def own_total(rows, qb, rc):
        own = (lax.rem(h, pairs) * 2 + h // pairs) * rows
        total = qb[pl.ds(pl.multiple_of(own, rows), rows), :]
        for n in range(2):
            total = total + rc[n].astype(F32).reshape(rows, LANES)
        return total

    stage_a(0, main_rows, q_main, sa_main, ra_main)
    round_wait(1)
    round_signal(2, 4)
    loads[5].wait()
    swaps[5].wait_recv()
    fill(q_gate, gate_rows, 0, mm(lhs, two(x_gate)))
    stage_a(1, gate_rows, q_gate, sa_gate, ra_gate)

    round_wait(2)
    arrived(ra_main, p_recv.at[0])
    stage_b(2, main_rows, q_main, ra_main, qb_main, sb_main, rb_main)
    arrived(ra_gate, p_recv.at[1])
    stage_b(3, gate_rows, q_gate, ra_gate, qb_gate, sb_gate, rb_gate)
    arrived(rb_main, p_recv.at[2])
    stage_c(4, main_rows, qb_main, rb_main, sc_main, rc_main)
    arrived(rb_gate, p_recv.at[3])
    stage_c(5, gate_rows, qb_gate, rb_gate, sc_gate, rc_gate)
    for i in range(11, 18):
        loads[i].wait()
    arrived(rc_main, p_recv.at[4])

    sums = own_total(main_rows, qb_main, rc_main)
    fresh = sums.astype(BF16).astype(F32)
    active = silu(base_rows[...] + fresh * tap_rows[(taps - 1) * main_rows : taps * main_rows, :])
    head_in = active[0:vec_rows]
    at = vec_rows + 2 * GROUPS
    step = (sums[at : at + 1, 0:heads] + sums[at + 1 : at + 2, 0:heads]).astype(BF16).astype(F32) + x_bias[...]
    step = jnp.maximum(step, 0.0) + jnp.log1p(jnp.exp(-jnp.abs(step)))
    kept = jnp.exp(-step * x_decay[...])
    low = iota((vec_rows, LANES), 1) < LANES // 2

    def by_channel(vector):
        rows = jnp.broadcast_to(vector, (vec_rows, heads))
        lane, at = iota((vec_rows, heads), 1), iota((vec_rows, heads), 0)
        first = jnp.sum(jnp.where(lane == 2 * at, rows, 0.0), axis=1, keepdims=True)
        second = jnp.sum(jnp.where(lane == 2 * at + 1, rows, 0.0), axis=1, keepdims=True)
        return jnp.where(low, first, second)

    turned = jnp.concatenate(
        [head_in * by_channel(step), by_channel(kept), jnp.zeros((LANES - 2 * vec_rows, LANES), F32)], axis=0
    ).T
    lane = iota((LANES, LANES), 1)
    readout = jnp.zeros((LANES, LANES), F32)
    per_group = vec_rows // GROUPS
    for r in range(vec_rows):
        g = vec_rows + r // per_group
        new = turned[:, vec_rows + r : vec_rows + r + 1] * x_state[r] + turned[:, r : r + 1] * active[g : g + 1]
        x_state[r] = new
        seen = jnp.sum(new * active[g + GROUPS : g + GROUPS + 1], axis=1, keepdims=True)
        readout = jnp.where(lane == r, seen, readout)
    state_out = pltpu.make_async_copy(x_state, o_state, out_sem.at[0])
    state_out.start()
    head_out = readout.T[0:vec_rows] + by_channel(x_skip[...]) * head_in
    arrived(rc_gate, p_recv.at[5])
    gated = head_out * silu(own_total(gate_rows, qb_gate, rc_gate).astype(BF16).astype(F32))
    scale = []
    for g in range(GROUPS):
        part = gated[g * per_group : (g + 1) * per_group]
        mean = jnp.sum(part * part, keepdims=True) / (per_group * LANES)
        scale.append(part * lax.rsqrt(mean + GATED_EPSILON))
    n_rows[z] = (jnp.concatenate(scale, axis=0) * x_ggain[...]).astype(BF16)

    def to_everyone(ref, i, source):
        def one(d):
            target = wrap(z + d, chips)
            send(source(target), ref.at[z], x_send.at[i], x_recv.at[i], target, c).start()

        one(half)

        def step_out(k, carry):
            one(half - 1 - k)
            one(chips - (half - 1 - k))
            return carry

        lax.fori_loop(0, half - 1, step_out, 0)

    def from_everyone(ref, i):
        arrived(ref.at[pl.ds(0, chips - 1)], x_recv.at[i])

    to_everyone(n_rows, 0, lambda target: n_rows.at[z])

    fresh_row[0 : taps - 2, :] = cache[1 : taps - 1]
    for k in range(conv_chunks):
        fresh_row[taps - 2 : taps - 1, k * LANES : (k + 1) * LANES] = fresh[k : k + 1]
    o_conv[0] = fresh_row[...].astype(BF16)
    own_tokens = one_hot(iota((chips, count), 1) == 2 * iota((chips, count), 0) + c)
    stream_cols = mm_nt(own_tokens, both)
    loads[6].wait()
    swaps[6].wait_recv()

    from_everyone(n_rows, 0)
    n_wide[...] = n_rows[...].astype(F32).reshape(chips * vec_rows, LANES)
    normed = jnp.concatenate(
        [n_wide[pl.ds(k, chips, stride=vec_rows), :] for k in range(vec_rows)], axis=1
    ).astype(BF16)
    mixed = mm_nt(normed, two(x_out)).astype(BF16).astype(F32)
    residual = RESIDUAL_SCALE * stream_cols + mixed
    r_rows[z] = jnp.concatenate([residual[: chips // 2], residual[chips // 2 :]], axis=1).astype(BF16)
    to_everyone(r_rows, 1, lambda target: r_rows.at[z])
    for i in range(18, len(loads)):
        loads[i].wait()
    from_everyone(r_rows, 1)

    chunks = chips // 2
    low = iota((chips // 2, LANES), 1) < LANES // 2
    total = jnp.zeros((chips, LANES), F32)
    square = jnp.zeros((chips, LANES), F32)
    for a in range(chunks):
        even, odd = r_rows[2 * a].astype(F32), r_rows[2 * a + 1].astype(F32)
        one = jnp.concatenate(
            [jnp.where(low, even, half_turn(odd)), jnp.where(low, half_turn(even), odd)], axis=0
        )
        res_s[a] = one
        total = total + one
        square = square + one * one
    width = chunks * LANES
    mean = jnp.sum(total, axis=1, keepdims=True) / width
    scale = lax.rsqrt(jnp.sum(square, axis=1, keepdims=True) / width - mean * mean + NORM_EPSILON)
    for a in range(chunks):
        first_s[c, a] = ((res_s[a] - mean) * scale * x_fgain[a : a + 1]).astype(BF16)
    swap = send(first_s.at[c], first_s.at[c], x_send.at[2], x_recv.at[2], z, 1 - c)
    swap.start()
    own_first = jnp.concatenate([first_s[c, a] for a in range(chunks)], axis=1)
    shared = (silu(mm(own_first, x_sg[...])) * mm(own_first, x_su[...])).astype(BF16)
    swap.wait_recv()

    everyone = jnp.concatenate(
        [jnp.concatenate([first_s[0, a], first_s[1, a]], axis=0) for a in range(chunks)], axis=1
    )
    taken = mm(chosen_s[...], everyone).astype(BF16)
    hidden = (silu(mm(taken, x_eg[0])) * mm(taken, x_eu[0])).astype(BF16)
    out = mm(hidden, x_ed[0])
    low = iota((CAP, LANES), 1) < LANES // 2
    per_tile = WINDOW // 2

    def joined(first, second, odd):
        if odd:
            return jnp.where(low, half_turn(first), second)
        return jnp.where(low, first, half_turn(second))

    for r in range(WINDOW):
        for j in range(chunks // (2 * per_tile)):
            at = (r // 2 + 2 * per_tile * j) * LANES
            other = at + per_tile * LANES
            s_exp[r, j] = joined(out[:, at : at + LANES], out[:, other : other + LANES], r % 2).astype(BF16)
    klass = lax.rem(z, WINDOW)
    to_everyone(r_exp, 3, lambda target: s_exp.at[lax.rem(target, WINDOW)])
    r_exp[z] = s_exp[klass]

    low = iota((chips, LANES), 1) < LANES // 2
    tiles = chunks // (2 * per_tile)
    for j in range(tiles):
        sides = []
        for i in (2 * j, 2 * j + 1):
            chunk = klass // 2 + per_tile * i
            part = mm(shared, x_sd[chunk]).astype(BF16).astype(F32)
            sides.append(part + RESIDUAL_SCALE * first_s[c, chunk].astype(F32))
        base_two[j] = jnp.where(p == 0, joined(*sides, 0), joined(*sides, 1))

    from_everyone(r_exp, 3)
    for j in range(tiles):
        rows = r_exp[:, j].astype(F32).reshape(chips * CAP, LANES).astype(BF16)
        part = mm(spread_s[...], rows)
        part = part[:count] + part[count:]
        for side in range(2):
            m_part[side, j] = part[side * chips : (side + 1) * chips]
    swap_two = send(m_part.at[1 - c], r_part, x_send.at[4], x_recv.at[4], z, 1 - c)
    swap_two.start()
    swap_two.wait_recv()
    second = [base_two[j] + m_part[c, j] + r_part[j] for j in range(tiles)]

    total = functools.reduce(lambda a, b: a + b, second)
    square = functools.reduce(lambda a, b: a + b, [s * s for s in second])
    lane = iota((chips, LANES), 1)
    sums = jnp.where(
        lane == 0,
        jnp.sum(total, axis=1, keepdims=True),
        jnp.where(lane == 1, jnp.sum(square, axis=1, keepdims=True), 0.0),
    )
    pad = jnp.zeros((LANES - chips, LANES), F32)
    stat_s[klass] = jnp.concatenate([sums, pad], axis=0).T[0:2]
    for d in (x for k in range(WINDOW // 2, 0, -1) for x in (k, -k) if x != -(WINDOW // 2)):
        send(stat_s.at[klass], stat_s.at[klass], x_send.at[5], x_recv.at[5], wrap(z + d, chips), c).start()
    arrived(stat_s.at[pl.ds(0, WINDOW - 1)], x_recv.at[5])
    sums = functools.reduce(lambda a, b: a + b, [stat_s[k] for k in range(WINDOW)])
    sums = jnp.concatenate([sums, jnp.zeros((LANES - 2, LANES), F32)], axis=0).T
    mean = sums[0:chips, 0:1] / width
    variance = sums[0:chips, 1:2] / width - mean * mean
    block = z // WINDOW
    own = second[0]
    for j in range(1, tiles):
        own = jnp.where(block // 2 == j, second[j], own)
    own = jnp.where(lax.rem(block, 2) == 0, own, half_turn(own))
    final_s[c] = (own - mean) * lax.rsqrt(variance + NORM_EPSILON)
    swap_three = send(final_s.at[c], final_s.at[c], x_send.at[6], x_recv.at[6], z, 1 - c)
    swap_three.start()
    cols = x_sgain.shape[1]
    gain = jnp.concatenate([x_sgain[...], jnp.zeros((1, LANES - cols), F32)], axis=1)
    row, col = iota((count, count), 0), iota((count, count), 1)
    back = one_hot(col == 2 * lax.rem(row, chips) + row // chips)
    take = one_hot(iota((cols, LANES), 0) == iota((cols, LANES), 1))
    swap_three.wait_recv()
    full = final_s[...].reshape(count, LANES)
    full = jnp.where(c == 0, full, pltpu.roll(full, LANES - cols, 1))
    full = (full * gain).astype(BF16)
    o_result[...] = mm(mm_nt(take, full).astype(BF16), back).astype(BF16)

    for copy in swaps + [swap, swap_two, swap_three]:
        copy.wait_send()
    for i, buffer in enumerate((sa_main, sa_gate, rb_main, rb_gate, rc_main, rc_gate)):
        arrived(buffer, p_send.at[i])
    for i, buffer in ((0, n_rows), (1, r_rows), (3, r_exp)):
        arrived(buffer.at[pl.ds(0, chips - 1)], x_send.at[i])
    arrived(stat_s.at[pl.ds(0, WINDOW - 1)], x_send.at[5])
    state_out.wait()


def on_device(
    chips,
    stream,
    conv_cache,
    scan_state,
    gate_weight,
    value_weight,
    entry_weight,
    readout_weight,
    step_weight,
    conv_weight,
    step_bias,
    decay_rate,
    skip_gain,
    group_gain,
    out_weight,
    first_gain,
    routes,
    route_weight,
    expert_gate,
    expert_up,
    expert_down,
    shared_gate,
    shared_up,
    shared_down,
    second_gain,
):
    heads = scan_state.shape[1]
    vec_rows = value_weight.shape[1] // LANES
    gate_rows = gate_weight.shape[1] // LANES
    main_rows = -(-(vec_rows + 2 * GROUPS + 2) // 8) * 8
    half, tokens = chips // 2, stream.shape[0]
    feats = stream.shape[1]
    width = feats * chips * 2
    chunks = width // LANES
    tiles = chunks // WINDOW
    operands = (
        stream.T,
        conv_cache,
        scan_state.reshape(-1, LANES, scan_state.shape[3]),
        gate_weight,
        value_weight,
        entry_weight,
        readout_weight,
        step_weight,
        conv_weight,
        step_bias[None],
        decay_rate[None],
        skip_gain[None],
        group_gain.reshape(-1, LANES),
        out_weight.T,
        first_gain.reshape(-1, LANES),
        routes.T,
        route_weight.T,
        expert_gate,
        expert_up,
        expert_down,
        shared_gate,
        shared_up,
        shared_down,
        second_gain[None],
    )
    doubled = (0, 3, 4, 5, 6, 7, 13)
    local = []
    for i, a in enumerate(operands):
        if i == 22:
            local.append(pltpu.VMEM((chunks, a.shape[0], LANES), a.dtype))
        else:
            local.append(pltpu.VMEM(((2,) if i in doubled else ()) + a.shape, a.dtype))

    def projection(rows):
        blocks = rows // 8
        return [
            pltpu.VMEM((chips * rows, LANES), F32),
            pltpu.VMEM((half, blocks, 8, LANES), BF16),
            pltpu.VMEM((half, blocks, 8, LANES), BF16),
            pltpu.VMEM((half * rows, LANES), F32),
            pltpu.VMEM((half // 2, 2, blocks, 8, LANES), BF16),
            pltpu.VMEM((half - 3, blocks, 8, LANES), BF16),
            pltpu.VMEM((2, blocks, 8, LANES), BF16),
            pltpu.VMEM((2, blocks, 8, LANES), BF16),
        ]

    taps = conv_weight.shape[0]
    scratch = (
        local
        + [
            pltpu.VMEM(((taps - 1) * main_rows, LANES), F32),
            pltpu.VMEM((taps * main_rows, LANES), F32),
            pltpu.VMEM((main_rows, LANES), F32),
            pltpu.VMEM((CAP, tokens), BF16),
            pltpu.VMEM((2 * tokens, chips * CAP), BF16),
        ]
        + projection(main_rows)
        + projection(gate_rows)
        + [
            pltpu.VMEM((taps - 1, conv_weight.shape[1]), F32),
            pltpu.VMEM((chips, vec_rows, LANES), BF16),
            pltpu.VMEM((chips * vec_rows, LANES), F32),
            pltpu.VMEM((chips, chips // 2, LANES), BF16),
            pltpu.VMEM((chunks, chips, LANES), F32),
            pltpu.VMEM((2, chunks, chips, LANES), BF16),
            pltpu.VMEM((WINDOW, tiles, CAP, LANES), BF16),
            pltpu.VMEM((chips, tiles, CAP, LANES), BF16),
            pltpu.VMEM((tiles, chips, LANES), F32),
            pltpu.VMEM((2, tiles, chips, LANES), F32),
            pltpu.VMEM((tiles, chips, LANES), F32),
            pltpu.VMEM((WINDOW, 2, LANES), F32),
            pltpu.VMEM((2, chips, LANES), F32),
            pltpu.SemaphoreType.DMA((len(operands) - 1 + chunks,)),
            pltpu.SemaphoreType.DMA((len(doubled),)),
            pltpu.SemaphoreType.DMA((len(doubled),)),
            pltpu.SemaphoreType.REGULAR((3,)),
            pltpu.SemaphoreType.DMA((6,)),
            pltpu.SemaphoreType.DMA((6,)),
            pltpu.SemaphoreType.DMA((7,)),
            pltpu.SemaphoreType.DMA((7,)),
            pltpu.SemaphoreType.DMA((1,)),
        ]
    )
    result, new_conv, new_state = pl.pallas_call(
        functools.partial(kernel, (chips, heads, vec_rows, main_rows, gate_rows)),
        out_shape=(
            jax.ShapeDtypeStruct((feats, tokens), BF16),
            jax.ShapeDtypeStruct(conv_cache.shape, BF16),
            jax.ShapeDtypeStruct(operands[2].shape, F32),
        ),
        in_specs=[pl.BlockSpec(memory_space=pl.ANY)] * len(operands),
        out_specs=(
            pl.BlockSpec(memory_space=pltpu.VMEM),
            pl.BlockSpec(memory_space=pltpu.VMEM),
            pl.BlockSpec(memory_space=pl.ANY),
        ),
        scratch_shapes=scratch,
        compiler_params=pltpu.CompilerParams(collective_id=0, has_side_effects=True, vmem_limit_bytes=50 * 2**20),
        name="step",
    )(*operands)
    return result.T, new_conv, new_state.reshape(scan_state.shape)


def solution(mesh):
    return jax.shard_map(
        functools.partial(on_device, mesh.shape["ep"] // 2),
        mesh=mesh,
        in_specs=(
            P("grp", "ep"),
            P(("grp", "ep"), None, None),
            P(("grp", "ep"), None, None, None),
            P("ep", None),
            P("ep", None),
            P("ep", None),
            P("ep", None),
            P("ep", None),
            P(),
            P(),
            P(),
            P(),
            P(),
            P(None, "ep"),
            P(),
            P("grp", None),
            P("grp", None),
            P("ep", None, None),
            P("ep", None, None),
            P("ep", None, None),
            P(),
            P(),
            P(),
            P("ep"),
        ),
        out_specs=(
            P("grp", "ep"),
            P(("grp", "ep"), None, None),
            P(("grp", "ep"), None, None, None),
        ),
        check_vma=False,
    )
```

time: 341 us -> 118 us (0.35)
  waiting for transfers between devices: 207 us -> 0 us
  Pallas kernels: 0 us -> 101 us
  blocking collectives: 54.9 us -> 0 us
  starting transfers between devices: 52.5 us -> 0 us
  other arithmetic: 8.58 us -> 0 us
  local copies, waits for them, and re-layouts: 8.24 us -> 16.3 us
  matrix products: 7.42 us -> 0 us
    all_to_all x4 -> x0, waiting for transfers between devices: 207 us -> none  [the longest x1 124 us: sent_and_summed(): lax.all_to_all(tiles, axis, split_axis=0, concat_axis=0, tiled=True)]
    pallas_call x0 -> x1, Pallas kernels: none -> 101 us  [on_device(): pl.pallas_call(functools.partial(kernel, (chips, heads, vec_rows, main_ro...]
    all_gather x1 -> x0, blocking collectives: 54.9 us -> none  [turned_gather(): lax.all_gather(both, axis, axis=0, tiled=True)]
    all_to_all x4 -> x0, starting transfers between devices: 52.5 us -> none  [the longest x1 34.5 us: sent_and_summed(): lax.all_to_all(tiles, axis, split_axis=0, concat_axis=0, tiled=True)]
    unnamed x44 -> x41, local copies, waits for them, and re-layouts: 2.8 us -> 16.3 us
    dot_general x12 -> x0, matrix products: 7.42 us -> none  [the longest x5 2.94 us: on_device(): jnp.dot(stream, weight, preferred_element_type=jnp.float32)]
  transfers between devices with their start and end apart: 4 -> 0, of which waited for: 4 -> 0; matrix products, arithmetic and copies ran while one was open for 1% -> 0% of each run, Pallas kernels for 0% -> 0%
where the time goes in v1:
time: 118 us
  Pallas kernels  101 us (86%)
  local copies, waits for them, and re-layouts  16.3 us (14%)
    pallas_call x1, Pallas kernels, on_device(): pl.pallas_call(functools.partial(kernel, (chips, heads, vec_rows, main_ro...  101 us
    unnamed x41, local copies, waits for them, and re-layouts  16.3 us

profile of v1, /device:TPU:37, one launch (start us, length us, event | category | flops | bytes accessed | tf_op | source)
XLA Modules:
  0.0 117.6 jit_solution(15244545373211807115)
XLA Ops:
  0.6 0.0 copy-start.5
  0.6 0.0 copy-start.15
  0.7 0.7 copy-done.5
  1.4 0.0 copy-done.15
  1.4 0.0 copy-start
  1.4 1.2 %copy-done = f32[1,32,64,128]{3,2,1,0:T(8,128)S(1)} copy-done((f32[1,32,64,128]{3,2,1,0:T(8,128)S(1)}, f32[1,32,64,128]{3,2,1,0:T(8,128)}, u32[]{:S(2)}) %copy-start) | copy-done | bytes 1048600
  2.6 0.0 copy-start.1
  2.6 1.2 %copy-done.1 = bf16[1,2048,256]{2,1,0:T(8,128)(2,1)S(1)} copy-done((bf16[1,2048,256]{2,1,0:T(8,128)(2,1)S(1)}, bf16[1,2048,256]{2,1,0:T(8,128)(2,1)}, u32[]{:S(2)}) %copy-start.1) | copy-done | bytes 1048600
  3.8 0.0 copy-start.2
  3.8 0.9 copy-done.2
  4.7 0.0 copy-start.3
  4.7 0.9 copy-done.3
  5.6 0.0 copy-start.4
  5.6 0.9 copy-done.4
  6.5 0.0 copy-start.6
  6.5 0.7 copy-done.6
  7.3 0.0 copy-start.7
  7.3 0.7 copy-done.7
  8.0 0.0 copy-start.8
  8.0 0.7 copy-done.8
  8.7 0.0 copy-start.9
  8.7 0.7 copy-done.9
  9.4 0.0 copy-start.10
  9.4 0.7 copy-done.10
  10.1 0.0 copy-start.11
  10.1 0.7 copy-done.11
  10.8 0.0 copy-start.12
  10.8 0.7 copy-done.12
  11.5 0.0 copy-start.13
  11.5 0.7 copy-done.13
  12.2 0.0 copy-start.14
  12.2 0.7 copy-done.14
  12.9 0.0 copy-start.16
  12.9 0.7 copy-done.16
  13.5 0.0 copy-start.17
  13.5 0.7 copy-done.17
  14.2 0.0 copy-start.18
  14.2 0.7 copy-done.18
  14.8 100.6 %step.1 = (bf16[32,64]{1,0:T(8,128)(2,1)S(1)}, bf16[1,3,2560]{2,1,0:T(4,128)(2,1)S(1)}, f32[16,128,128]{2,1,0:T(8,128)S(1)}) custom-call(bf16[32,64]{1,0:T(8,128)(2,1)S(1)} %bitcast.16, bf16[1,3,2560]{2,1,0:T(4,128)(2,1)S(1)} %copy-done.5, f32[16,128,128]{2,1,0:T(8,128)S(1)} %bitcast.13, bf16[32,2048]{1,0:T(8,128)(2,1)S(1)} %copy-done.2, ...), custom_call_target="tpu_custom_call" | custom-call | tf_op jit(solution)/shard_map/step/pallas_call | solution.py:590
  115.4 0.6 copy.30
  116.0 0.6 copy.31
  116.6 1.0 copy.32
Async XLA Ops:
  0.6 0.7 copy-start.5
  0.6 0.7 copy-start.15
  1.4 1.2 %copy-start = (f32[1,32,64,128]{3,2,1,0:T(8,128)S(1)}, f32[1,32,64,128]{3,2,1,0:T(8,128)}, u32[]{:S(2)}) copy-start(f32[1,32,64,128]{3,2,1,0:T(8,128)} %param.26) | copy-start | bytes 3145732
  2.6 1.2 %copy-start.1 = (bf16[1,2048,256]{2,1,0:T(8,128)(2,1)S(1)}, bf16[1,2048,256]{2,1,0:T(8,128)(2,1)}, u32[]{:S(2)}) copy-start(bf16[1,2048,256]{2,1,0:T(8,128)(2,1)} %refs_17_.1) | copy-start | bytes 3145732
  3.8 0.9 copy-start.2
  4.7 0.9 copy-start.3
  5.6 0.9 copy-start.4
  6.5 0.7 copy-start.6
  7.3 0.7 copy-start.7
  8.0 0.7 copy-start.8
  8.7 0.7 copy-start.9
  9.4 0.7 copy-start.10
  10.1 0.7 copy-start.11
  10.8 0.7 copy-start.12
  11.5 0.7 copy-start.13
  12.2 0.7 copy-start.14
  12.9 0.7 copy-start.16
  13.5 0.7 copy-start.17
  14.2 0.7 copy-start.18

commit v2 on v1

--- a/solution.py
+++ b/solution.py
@@ -594,14 +594,14 @@
             jax.ShapeDtypeStruct(conv_cache.shape, BF16),
             jax.ShapeDtypeStruct(operands[2].shape, F32),
         ),
-        in_specs=[pl.BlockSpec(memory_space=pl.ANY)] * len(operands),
+        in_specs=[pl.BlockSpec(memory_space=pltpu.HBM)] * len(operands),
         out_specs=(
             pl.BlockSpec(memory_space=pltpu.VMEM),
             pl.BlockSpec(memory_space=pltpu.VMEM),
-            pl.BlockSpec(memory_space=pl.ANY),
+            pl.BlockSpec(memory_space=pltpu.HBM),
         ),
         scratch_shapes=scratch,
-        compiler_params=pltpu.CompilerParams(collective_id=0, has_side_effects=True, vmem_limit_bytes=50 * 2**20),
+        compiler_params=pltpu.CompilerParams(collective_id=0, has_side_effects=True, vmem_limit_bytes=67043328),
         name="step",
     )(*operands)
     return result.T, new_conv, new_state.reshape(scan_state.shape)

time: 118 us -> 107 us (0.907)
  local copies, waits for them, and re-layouts: 16.3 us -> 4.22 us
    unnamed x41 -> x5, local copies, waits for them, and re-layouts: 16.3 us -> 4.22 us
where the time goes in v2:
time: 107 us; the launch traced here: 106 us
  Pallas kernels  102 us (95%)
  local copies, waits for them, and re-layouts  4.22 us (4%)
    pallas_call x1, Pallas kernels, on_device(): pl.pallas_call(functools.partial(kernel, (chips, heads, vec_rows, main_ro...  102 us
    unnamed x5, local copies, waits for them, and re-layouts  4.22 us

profile of v2, /device:TPU:37, one launch (start us, length us, event | category | flops | bytes accessed | tf_op | source)
XLA Modules:
  0.0 106.5 jit_solution(14997942340005390260)
XLA Ops:
  0.6 101.6 %step.1 = (bf16[32,64]{1,0:T(8,128)(2,1)}, bf16[1,3,2560]{2,1,0:T(4,128)(2,1)}, f32[16,128,128]{2,1,0:T(8,128)}) custom-call(bf16[32,64]{1,0:T(8,128)(2,1)} %bitcast.16, bf16[1,3,2560]{2,1,0:T(4,128)(2,1)} %refs_1_.1, f32[16,128,128]{2,1,0:T(8,128)} %bitcast.13, bf16[32,2048]{1,0:T(8,128)(2,1)} %refs_3_.1, bf16[32,2048]{1,0:T(8,128)(2,1)} %refs_4_.1, ...), custom_call_target="tpu_custom_call" | custom-call | tf_op jit(solution)/shard_map/step/pallas_call | solution.py:590
  102.2 0.0 copy-start
  102.2 1.3 %copy.30 = bf16[64,32]{0,1:T(8,128)(2,1)} copy(bf16[64,32]{0,1:T(8,128)(2,1)} %bitcast.19) | data formatting | bytes 8192
  103.5 0.0 copy-done
  103.6 0.6 copy.31
  104.2 2.3 %copy.32 = f32[1,32,64,128]{3,2,1,0:T(8,128)} copy(f32[1,32,64,128]{3,2,1,0:T(8,128)} %bitcast.14) | data formatting | bytes 2097152
Async XLA Ops:
  102.2 1.3 %copy-start = (bf16[1,3,2560]{2,1,0:T(4,128)(2,1)S(1)}, bf16[1,3,2560]{2,1,0:T(4,128)(2,1)}, u32[]{:S(2)}) copy-start(bf16[1,3,2560]{2,1,0:T(4,128)(2,1)} %get-tuple-element.13) | copy-start | bytes 46084

commit v3 on v2

--- a/solution.py
+++ b/solution.py
@@ -52,10 +52,10 @@
         x_stream, x_cache, x_state, x_gate, x_value, x_entry, x_readout, x_step, x_conv_w, x_bias, x_decay, x_skip,
         x_ggain, x_out, x_fgain, x_routes, x_route_w, x_eg, x_eu, x_ed, x_sg, x_su, x_sd, x_sgain,
         conv_rows, tap_rows, base_rows, chosen_s, spread_s,
-        q_main, sa_main, ra_main, qb_main, sb_main, rb_main, sc_main, rc_main,
-        q_gate, sa_gate, ra_gate, qb_gate, sb_gate, rb_gate, sc_gate, rc_gate,
+        q_main, sa_main, ra_main, qb_main, sb_main, rb_main, sc_main, rc_main, so_main,
+        q_gate, sa_gate, ra_gate, qb_gate, sb_gate, rb_gate, sc_gate, rc_gate, so_gate,
         fresh_row, n_rows, n_wide, r_rows, res_s, first_s, s_exp, r_exp, base_two, m_part, r_part, stat_s, final_s,
-        local_sem, sib_sem, ssib_sem, round_sem, p_send, p_recv, x_send, x_recv, out_sem,
+        local_sem, sib_sem, ssib_sem, round_sem, p_send, p_recv, rc_sem, x_send, x_recv, out_sem,
     ) = refs
     me = lax.axis_index("ep")
     z, c = me // 2, lax.rem(me, 2)
@@ -86,29 +86,60 @@
     signal(barrier, wrap(z + 1, chips), c)
     signal(barrier, wrap(z - 1, chips), c)
 
-    shared_in = ((stream, x_stream), (w_value, x_value), (w_entry, x_entry), (w_readout, x_readout), (w_step, x_step),
-                 (w_gate, x_gate), (w_out, x_out))
-    loads = []
-    for src, dst in shared_in:
-        loads.append((src, dst.at[c]))
-    for pair in (
+    main_in = ((w_value, x_value), (w_entry, x_entry), (w_readout, x_readout), (w_step, x_step))
+    gate_in = ((w_gate, x_gate),)
+    both_in = ((stream, x_stream), (second_gain, x_sgain), (w_out, x_out))
+
+    def load(i, src, dst):
+        return pltpu.make_async_copy(src, dst, local_sem.at[i])
+
+    own_in = [load(i, src, dst.at[c]) for i, (src, dst) in enumerate(both_in)]
+    main_own = [load(3 + i, src, dst.at[c]) for i, (src, dst) in enumerate(main_in)]
+    gate_own = [load(3 + i, src, dst.at[c]) for i, (src, dst) in enumerate(gate_in)]
+    loads = [
         (conv_cache, x_cache), (conv_w, x_conv_w), (routes, x_routes), (route_w, x_route_w), (step_bias, x_bias),
-        (decay, x_decay), (skip, x_skip), (group_gain, x_ggain), (first_gain, x_fgain), (second_gain, x_sgain),
-        (state_in, x_state), (e_gate, x_eg), (e_up, x_eu), (e_down, x_ed), (s_gate, x_sg), (s_up, x_su),
-    ):
-        loads.append(pair)
-    chunks_d = x_sd.shape[0]
-    for k in range(chunks_d):
+        (decay, x_decay), (skip, x_skip), (group_gain, x_ggain), (state_in, x_state), (first_gain, x_fgain),
+        (e_gate, x_eg), (e_up, x_eu), (e_down, x_ed), (s_gate, x_sg), (s_up, x_su),
+    ]
+    for k in range(x_sd.shape[0]):
         loads.append((s_down.at[:, pl.ds(k * LANES, LANES)], x_sd.at[k]))
-    loads = [pltpu.make_async_copy(s, d, local_sem.at[i]) for i, (s, d) in enumerate(loads)]
-    for copy in loads:
+    loads = [load(7 + i, src, dst) for i, (src, dst) in enumerate(loads)]
+    own_in[0].start()
+
+    @pl.when(c == 1)
+    def _():
+        for copy in main_own:
+            copy.start()
+
+    @pl.when(c == 0)
+    def _():
+        for copy in gate_own:
+            copy.start()
+
+    for copy in own_in[1:] + loads:
         copy.start()
 
     pl.semaphore_wait(barrier, 3)
-    swaps = [
-        send(src, dst.at[c], ssib_sem.at[i], sib_sem.at[i], z, 1 - c) for i, (src, dst) in enumerate(shared_in)
-    ]
-    for copy in swaps:
+
+    def swap(i, src, dst):
+        return send(src, dst.at[c], ssib_sem.at[i], sib_sem.at[i], z, 1 - c)
+
+    both_swaps = [swap(i, src, dst) for i, (src, dst) in enumerate(both_in)]
+    main_swaps = [swap(3 + i, src, dst) for i, (src, dst) in enumerate(main_in)]
+    gate_swaps = [swap(3 + i, src, dst) for i, (src, dst) in enumerate(gate_in)]
+    both_swaps[0].start()
+
+    @pl.when(c == 0)
+    def _():
+        for copy in main_swaps:
+            copy.start()
+
+    @pl.when(c == 1)
+    def _():
+        for copy in gate_swaps:
+            copy.start()
+
+    for copy in both_swaps[1:]:
         copy.start()
 
     def round_signal(i, d):
@@ -121,7 +152,7 @@
     round_signal(0, 1)
 
     count = x_routes.shape[1]
-    for i in (7, 8, 9, 10):
+    for i in (0, 1, 2, 3):
         loads[i].wait()
     expert_of = iota((2 * chips, count), 0)
     member, weight = jnp.zeros((2 * chips, count), F32), jnp.zeros((2 * chips, count), F32)
@@ -165,31 +196,20 @@
 
     round_wait(0)
     round_signal(1, 2)
-    for i in range(5):
-        loads[i].wait()
-        swaps[i].wait_recv()
+    own_in[0].wait()
+    both_swaps[0].wait_recv()
     both = x_stream[...].reshape(-1, count)
-    row, col = iota((chips, count), 0), iota((chips, count), 1)
-    within = lax.rem(row, half)
-    chip_of = 2 * (within // 2 + pairs * lax.rem(within, 2)) + row // half
-    lhs = mm_nt(one_hot(col == 2 * chip_of + c), both).astype(BF16)
+    row, col = iota((count, count), 0), iota((count, count), 1)
+    within = lax.rem(row // 2, half)
+    chip_of = 2 * (within // 2 + pairs * lax.rem(within, 2)) + row // (2 * half)
+    lhs = mm_nt(one_hot(col == 2 * chip_of + lax.rem(row, 2)), both).astype(BF16)
 
     def two(ref):
         return ref[...].reshape(-1, ref.shape[-1])
 
     def fill(q, rows, first, product):
         for k in range(product.shape[1] // LANES):
-            q[pl.ds(first + k, chips, stride=rows), :] = product[:, k * LANES : (k + 1) * LANES]
-
-    zero = jnp.zeros((chips, LANES), F32)
-    fill(q_main, main_rows, 0, mm(lhs, two(x_value)))
-    fill(q_main, main_rows, vec_rows, mm(lhs, two(x_entry)))
-    fill(q_main, main_rows, vec_rows + GROUPS, mm(lhs, two(x_readout)))
-    steps = mm(lhs, two(x_step))
-    steps = jnp.concatenate([steps, zero[:, : LANES - steps.shape[1]]], axis=1)
-    fill(q_main, main_rows, vec_rows + 2 * GROUPS, steps)
-    for k in range(vec_rows + 2 * GROUPS + 1, main_rows):
-        fill(q_main, main_rows, k, zero)
+            q[pl.ds(first + k, count, stride=rows), :] = product[:, k * LANES : (k + 1) * LANES]
 
     across = z + 1 - 2 * p
     step_at = (vec_rows + 2 * GROUPS) % 8
@@ -205,73 +225,86 @@
         tail = jnp.where(at == step_at, near, jnp.where(at == step_at + 1, whole - near, tail))
         return jnp.concatenate([blocks[:, :-1], tail[:, None]], axis=1).astype(BF16)
 
-    def stage_a(i, rows, q, sa, ra):
-        start = pl.multiple_of((1 - p) * half * rows, half * rows)
-        sa[...] = to_send(q[pl.ds(start, half * rows), :], half, rows)
-        copy = send(sa, ra, p_send.at[i], p_recv.at[i], across, c)
-        copy.start()
-        return copy
-
-    def stage_b(i, rows, q, ra, qb, sb, rb):
-        start = pl.multiple_of(p * half * rows, half * rows)
-        total = q[pl.ds(start, half * rows), :] + ra[...].astype(F32).reshape(half * rows, LANES)
+    minus = wrap(h - quarter, half) // pairs
+
+    def reduce_columns(kind, rows, q, sa, ra, qb, sb, rb, sc, rc, so):
+        size = 2 * half * rows
+        start = pl.multiple_of((1 - p) * size, size)
+        sa[...] = to_send(q[pl.ds(start, size), :], 2 * half, rows)
+        send(sa, ra, p_send.at[0], p_recv.at[0], across, c).start()
+        round_wait(1)
+        round_signal(2, 4)
+        round_wait(2)
+        arrived(ra, p_recv.at[0])
+        start = pl.multiple_of(p * size, size)
+        total = q[pl.ds(start, size), :] + ra[...].astype(F32).reshape(size, LANES)
         qb[...] = total
-        sb[...] = to_send(total, half, rows).reshape(sb.shape)
+        sb[...] = to_send(total, 2 * half, rows).reshape(sb.shape)
         u, v = lax.rem(h, pairs), h // pairs
         target = 2 * wrap(h - quarter, half) + p
         last = rb.shape[0] - 1
-        copies = [send(sb.at[u, 1 - v], rb.at[last], p_send.at[i], p_recv.at[i], target, c)]
+        copies = [send(sb.at[u, 1 - v], rb.at[last], p_send.at[1], p_recv.at[1], target, c)]
         for n, e in enumerate(x for k in range(quarter - 1, 0, -1) for x in (k, -k)):
             u = lax.rem(h + e + quarter + half, pairs)
             target = 2 * wrap(h + e, half) + p
-            copies.append(send(sb.at[u], rb.at[pl.ds(2 * n, 2)], p_send.at[i], p_recv.at[i], target, c))
+            copies.append(send(sb.at[u], rb.at[pl.ds(2 * n, 2)], p_send.at[1], p_recv.at[1], target, c))
         for copy in copies:
             copy.start()
-
-    minus = wrap(h - quarter, half) // pairs
-
-    def stage_c(i, rows, qb, rb, sc, rc):
-        u = lax.rem(h + quarter, pairs)
-        start = pl.multiple_of(u * 2 * rows, 2 * rows)
-        total = qb[pl.ds(start, 2 * rows), :].reshape(2, rows, LANES)
-        last = rb.shape[0] - 1
+        at = pl.multiple_of((lax.rem(h, pairs) * 2 + h // pairs) * 2 * rows, 2 * rows)
+        so[...] = to_send(qb[pl.ds(at, 2 * rows), :], 2, rows)
+        rc[2] = so[c]
+        send(so.at[1 - c], rc.at[2], p_send.at[3], rc_sem.at[kind], z, 1 - c).start()
+        arrived(rb, p_recv.at[1])
+        at = pl.multiple_of(lax.rem(h + quarter, pairs) * 4 * rows, 4 * rows)
+        total = qb[pl.ds(at, 4 * rows), :].reshape(2, 2 * rows, LANES)
         for n in range(0, last, 2):
-            total = total + rb[n : n + 2].astype(F32).reshape(2, rows, LANES)
-        extra = rb[last].astype(F32).reshape(rows, LANES)
+            total = total + rb[n : n + 2].astype(F32).reshape(2, 2 * rows, LANES)
+        extra = rb[last].astype(F32).reshape(2 * rows, LANES)
         for v in range(2):
-            sc[v] = to_send(total[v] + jnp.where(minus == v, extra, 0.0), 1, rows)[0]
+            sc[v] = to_send(total[v] + jnp.where(minus == v, extra, 0.0), 2, rows)
         for n, (v, target) in enumerate(((minus, h - quarter), (1 - minus, h + quarter))):
-            send(sc.at[v], rc.at[n], p_send.at[i], p_recv.at[i], 2 * wrap(target, half) + p, c).start()
-
-    def own_total(rows, qb, rc):
-        own = (lax.rem(h, pairs) * 2 + h // pairs) * rows
-        total = qb[pl.ds(pl.multiple_of(own, rows), rows), :]
-        for n in range(2):
-            total = total + rc[n].astype(F32).reshape(rows, LANES)
-        return total
-
-    stage_a(0, main_rows, q_main, sa_main, ra_main)
-    round_wait(1)
-    round_signal(2, 4)
-    loads[5].wait()
-    swaps[5].wait_recv()
-    fill(q_gate, gate_rows, 0, mm(lhs, two(x_gate)))
-    stage_a(1, gate_rows, q_gate, sa_gate, ra_gate)
-
-    round_wait(2)
-    arrived(ra_main, p_recv.at[0])
-    stage_b(2, main_rows, q_main, ra_main, qb_main, sb_main, rb_main)
-    arrived(ra_gate, p_recv.at[1])
-    stage_b(3, gate_rows, q_gate, ra_gate, qb_gate, sb_gate, rb_gate)
-    arrived(rb_main, p_recv.at[2])
-    stage_c(4, main_rows, qb_main, rb_main, sc_main, rc_main)
-    arrived(rb_gate, p_recv.at[3])
-    stage_c(5, gate_rows, qb_gate, rb_gate, sc_gate, rc_gate)
-    for i in range(11, 18):
+            for core in range(2):
+                send(
+                    sc.at[v, core], rc.at[n], p_send.at[2], rc_sem.at[kind], 2 * wrap(target, half) + p, core
+                ).start()
+
+    main_bufs = (q_main, sa_main, ra_main, qb_main, sb_main, rb_main, sc_main, rc_main, so_main)
+    gate_bufs = (q_gate, sa_gate, ra_gate, qb_gate, sb_gate, rb_gate, sc_gate, rc_gate, so_gate)
+
+    @pl.when(c == 1)
+    def _():
+        for i in range(len(main_in)):
+            main_own[i].wait()
+            main_swaps[i].wait_recv()
+        zero = jnp.zeros((count, LANES), F32)
+        fill(q_main, main_rows, 0, mm(lhs, two(x_value)))
+        fill(q_main, main_rows, vec_rows, mm(lhs, two(x_entry)))
+        fill(q_main, main_rows, vec_rows + GROUPS, mm(lhs, two(x_readout)))
+        steps = mm(lhs, two(x_step))
+        steps = jnp.concatenate([steps, zero[:, : LANES - steps.shape[1]]], axis=1)
+        fill(q_main, main_rows, vec_rows + 2 * GROUPS, steps)
+        for k in range(vec_rows + 2 * GROUPS + 1, main_rows):
+            fill(q_main, main_rows, k, zero)
+        reduce_columns(0, main_rows, *main_bufs)
+        arrived(rc_main.at[pl.ds(0, 2)], rc_sem.at[0])
+
+    @pl.when(c == 0)
+    def _():
+        for i in range(len(gate_in)):
+            gate_own[i].wait()
+            gate_swaps[i].wait_recv()
+        fill(q_gate, gate_rows, 0, mm(lhs, two(x_gate)))
+        reduce_columns(1, gate_rows, *gate_bufs)
+        arrived(rc_main, rc_sem.at[0])
+
+    for i in range(4, 9):
         loads[i].wait()
-    arrived(rc_main, p_recv.at[4])
-
-    sums = own_total(main_rows, qb_main, rc_main)
+
+    def own_total(rows, rc):
+        total = rc[0].astype(F32) + rc[1].astype(F32) + rc[2].astype(F32)
+        return total.reshape(rows, LANES)
+
+    sums = own_total(main_rows, rc_main)
     fresh = sums.astype(BF16).astype(F32)
     active = silu(base_rows[...] + fresh * tap_rows[(taps - 1) * main_rows : taps * main_rows, :])
     head_in = active[0:vec_rows]
@@ -289,22 +322,31 @@
         return jnp.where(low, first, second)
 
     turned = jnp.concatenate(
-        [head_in * by_channel(step), by_channel(kept), jnp.zeros((LANES - 2 * vec_rows, LANES), F32)], axis=0
+        [head_in * by_channel(step), jnp.zeros((LANES - vec_rows, LANES), F32)], axis=0
     ).T
+    top = iota((LANES, LANES), 0) < LANES // 2
     lane = iota((LANES, LANES), 1)
     readout = jnp.zeros((LANES, LANES), F32)
     per_group = vec_rows // GROUPS
     for r in range(vec_rows):
         g = vec_rows + r // per_group
-        new = turned[:, vec_rows + r : vec_rows + r + 1] * x_state[r] + turned[:, r : r + 1] * active[g : g + 1]
+        keep = jnp.where(top, kept[:, 2 * r : 2 * r + 1], kept[:, 2 * r + 1 : 2 * r + 2])
+        new = keep * x_state[r] + turned[:, r : r + 1] * active[g : g + 1]
         x_state[r] = new
         seen = jnp.sum(new * active[g + GROUPS : g + GROUPS + 1], axis=1, keepdims=True)
         readout = jnp.where(lane == r, seen, readout)
     state_out = pltpu.make_async_copy(x_state, o_state, out_sem.at[0])
     state_out.start()
     head_out = readout.T[0:vec_rows] + by_channel(x_skip[...]) * head_in
-    arrived(rc_gate, p_recv.at[5])
-    gated = head_out * silu(own_total(gate_rows, qb_gate, rc_gate).astype(BF16).astype(F32))
+    @pl.when(c == 0)
+    def _():
+        arrived(rc_gate.at[pl.ds(0, 2)], rc_sem.at[1])
+
+    @pl.when(c == 1)
+    def _():
+        arrived(rc_gate, rc_sem.at[1])
+
+    gated = head_out * silu(own_total(gate_rows, rc_gate).astype(BF16).astype(F32))
     scale = []
     for g in range(GROUPS):
         part = gated[g * per_group : (g + 1) * per_group]
@@ -337,8 +379,9 @@
     o_conv[0] = fresh_row[...].astype(BF16)
     own_tokens = one_hot(iota((chips, count), 1) == 2 * iota((chips, count), 0) + c)
     stream_cols = mm_nt(own_tokens, both)
-    loads[6].wait()
-    swaps[6].wait_recv()
+    for i in (1, 2):
+        own_in[i].wait()
+        both_swaps[i].wait_recv()
 
     from_everyone(n_rows, 0)
     n_wide[...] = n_rows[...].astype(F32).reshape(chips * vec_rows, LANES)
@@ -349,7 +392,7 @@
     residual = RESIDUAL_SCALE * stream_cols + mixed
     r_rows[z] = jnp.concatenate([residual[: chips // 2], residual[chips // 2 :]], axis=1).astype(BF16)
     to_everyone(r_rows, 1, lambda target: r_rows.at[z])
-    for i in range(18, len(loads)):
+    for i in range(9, len(loads)):
         loads[i].wait()
     from_everyone(r_rows, 1)
 
@@ -370,11 +413,11 @@
     scale = lax.rsqrt(jnp.sum(square, axis=1, keepdims=True) / width - mean * mean + NORM_EPSILON)
     for a in range(chunks):
         first_s[c, a] = ((res_s[a] - mean) * scale * x_fgain[a : a + 1]).astype(BF16)
-    swap = send(first_s.at[c], first_s.at[c], x_send.at[2], x_recv.at[2], z, 1 - c)
-    swap.start()
+    swap_one = send(first_s.at[c], first_s.at[c], x_send.at[2], x_recv.at[2], z, 1 - c)
+    swap_one.start()
     own_first = jnp.concatenate([first_s[c, a] for a in range(chunks)], axis=1)
     shared = (silu(mm(own_first, x_sg[...])) * mm(own_first, x_su[...])).astype(BF16)
-    swap.wait_recv()
+    swap_one.wait_recv()
 
     everyone = jnp.concatenate(
         [jnp.concatenate([first_s[0, a], first_s[1, a]], axis=0) for a in range(chunks)], axis=1
@@ -430,40 +473,65 @@
         jnp.where(lane == 1, jnp.sum(square, axis=1, keepdims=True), 0.0),
     )
     pad = jnp.zeros((LANES - chips, LANES), F32)
-    stat_s[klass] = jnp.concatenate([sums, pad], axis=0).T[0:2]
-    for d in (x for k in range(WINDOW // 2, 0, -1) for x in (k, -k) if x != -(WINDOW // 2)):
-        send(stat_s.at[klass], stat_s.at[klass], x_send.at[5], x_recv.at[5], wrap(z + d, chips), c).start()
-    arrived(stat_s.at[pl.ds(0, WINDOW - 1)], x_recv.at[5])
-    sums = functools.reduce(lambda a, b: a + b, [stat_s[k] for k in range(WINDOW)])
-    sums = jnp.concatenate([sums, jnp.zeros((LANES - 2, LANES), F32)], axis=0).T
-    mean = sums[0:chips, 0:1] / width
-    variance = sums[0:chips, 1:2] / width - mean * mean
+    stat_s[c, klass] = jnp.concatenate([sums, pad], axis=0).T[0:2]
+    own_stat = stat_s.at[c, klass]
+    near = [x for k in range(WINDOW // 2, 0, -1) for x in (k, -k) if x != -(WINDOW // 2)]
+    for d in near:
+        for core in range(2):
+            send(own_stat, own_stat, x_send.at[5], x_recv.at[5], wrap(z + d, chips), core).start()
+    send(own_stat, own_stat, x_send.at[5], x_recv.at[5], z, 1 - c).start()
     block = z // WINDOW
     own = second[0]
     for j in range(1, tiles):
         own = jnp.where(block // 2 == j, second[j], own)
-    own = jnp.where(lax.rem(block, 2) == 0, own, half_turn(own))
-    final_s[c] = (own - mean) * lax.rsqrt(variance + NORM_EPSILON)
+    final_s[c] = jnp.where(lax.rem(block, 2) == 0, own, half_turn(own))
     swap_three = send(final_s.at[c], final_s.at[c], x_send.at[6], x_recv.at[6], z, 1 - c)
     swap_three.start()
-    cols = x_sgain.shape[1]
-    gain = jnp.concatenate([x_sgain[...], jnp.zeros((1, LANES - cols), F32)], axis=1)
+    cols = x_sgain.shape[2]
+    gain = jnp.concatenate([x_sgain[c], jnp.zeros((1, LANES - cols), F32)], axis=1)
     row, col = iota((count, count), 0), iota((count, count), 1)
     back = one_hot(col == 2 * lax.rem(row, chips) + row // chips)
     take = one_hot(iota((cols, LANES), 0) == iota((cols, LANES), 1))
     swap_three.wait_recv()
     full = final_s[...].reshape(count, LANES)
     full = jnp.where(c == 0, full, pltpu.roll(full, LANES - cols, 1))
+    stat_wait = stat_s.reshape(2 * WINDOW, 2, LANES).at[pl.ds(0, 2 * WINDOW - 1)]
+    arrived(stat_wait, x_recv.at[5])
+    mean, variance = [], []
+    for core in range(2):
+        sums = functools.reduce(lambda a, b: a + b, [stat_s[core, k] for k in range(WINDOW)])
+        sums = jnp.concatenate([sums, jnp.zeros((LANES - 2, LANES), F32)], axis=0).T
+        mean.append(sums[0:chips, 0:1] / width)
+        variance.append(sums[0:chips, 1:2] / width - mean[core] * mean[core])
+    mean, variance = jnp.concatenate(mean, axis=0), jnp.concatenate(variance, axis=0)
+    full = (full - mean) * lax.rsqrt(variance + NORM_EPSILON)
     full = (full * gain).astype(BF16)
     o_result[...] = mm(mm_nt(take, full).astype(BF16), back).astype(BF16)
 
-    for copy in swaps + [swap, swap_two, swap_three]:
+    for copy in both_swaps + [swap_one, swap_two, swap_three]:
         copy.wait_send()
-    for i, buffer in enumerate((sa_main, sa_gate, rb_main, rb_gate, rc_main, rc_gate)):
-        arrived(buffer, p_send.at[i])
+
+    def left(rb, sa, sc, so):
+        arrived(sa, p_send.at[0])
+        arrived(rb, p_send.at[1])
+        arrived(sc, p_send.at[2])
+        arrived(so.at[0], p_send.at[3])
+
+    @pl.when(c == 1)
+    def _():
+        for copy in gate_swaps:
+            copy.wait_send()
+        left(rb_main, sa_main, sc_main, so_main)
+
+    @pl.when(c == 0)
+    def _():
+        for copy in main_swaps:
+            copy.wait_send()
+        left(rb_gate, sa_gate, sc_gate, so_gate)
+
     for i, buffer in ((0, n_rows), (1, r_rows), (3, r_exp)):
         arrived(buffer.at[pl.ds(0, chips - 1)], x_send.at[i])
-    arrived(stat_s.at[pl.ds(0, WINDOW - 1)], x_send.at[5])
+    arrived(stat_wait, x_send.at[5])
     state_out.wait()
 
 
@@ -529,7 +597,7 @@
         shared_down,
         second_gain[None],
     )
-    doubled = (0, 3, 4, 5, 6, 7, 13)
+    doubled = (0, 3, 4, 5, 6, 7, 13, 23)
     local = []
     for i, a in enumerate(operands):
         if i == 22:
@@ -538,16 +606,17 @@
             local.append(pltpu.VMEM(((2,) if i in doubled else ()) + a.shape, a.dtype))
 
     def projection(rows):
-        blocks = rows // 8
+        block = (rows // 8, 8, LANES)
         return [
+            pltpu.VMEM((tokens * rows, LANES), F32),
+            pltpu.VMEM((chips, *block), BF16),
+            pltpu.VMEM((chips, *block), BF16),
             pltpu.VMEM((chips * rows, LANES), F32),
-            pltpu.VMEM((half, blocks, 8, LANES), BF16),
-            pltpu.VMEM((half, blocks, 8, LANES), BF16),
-            pltpu.VMEM((half * rows, LANES), F32),
-            pltpu.VMEM((half // 2, 2, blocks, 8, LANES), BF16),
-            pltpu.VMEM((half - 3, blocks, 8, LANES), BF16),
-            pltpu.VMEM((2, blocks, 8, LANES), BF16),
-            pltpu.VMEM((2, blocks, 8, LANES), BF16),
+            pltpu.VMEM((half // 2, 2, 2, *block), BF16),
+            pltpu.VMEM((half - 3, 2, *block), BF16),
+            pltpu.VMEM((2, 2, *block), BF16),
+            pltpu.VMEM((3, *block), BF16),
+            pltpu.VMEM((2, *block), BF16),
         ]
 
     taps = conv_weight.shape[0]
@@ -574,14 +643,15 @@
             pltpu.VMEM((tiles, chips, LANES), F32),
             pltpu.VMEM((2, tiles, chips, LANES), F32),
             pltpu.VMEM((tiles, chips, LANES), F32),
-            pltpu.VMEM((WINDOW, 2, LANES), F32),
+            pltpu.VMEM((2, WINDOW, 2, LANES), F32),
             pltpu.VMEM((2, chips, LANES), F32),
             pltpu.SemaphoreType.DMA((len(operands) - 1 + chunks,)),
-            pltpu.SemaphoreType.DMA((len(doubled),)),
-            pltpu.SemaphoreType.DMA((len(doubled),)),
+            pltpu.SemaphoreType.DMA((7,)),
+            pltpu.SemaphoreType.DMA((7,)),
             pltpu.SemaphoreType.REGULAR((3,)),
-            pltpu.SemaphoreType.DMA((6,)),
-            pltpu.SemaphoreType.DMA((6,)),
+            pltpu.SemaphoreType.DMA((4,)),
+            pltpu.SemaphoreType.DMA((2,)),
+            pltpu.SemaphoreType.DMA((2,)),
             pltpu.SemaphoreType.DMA((7,)),
             pltpu.SemaphoreType.DMA((7,)),
             pltpu.SemaphoreType.DMA((1,)),

time: 107 us -> 112 us (1.047)
  Pallas kernels: 102 us -> 107 us
    pallas_call x1, Pallas kernels: 102 us -> 107 us  [on_device(): pl.pallas_call(functools.partial(kernel, (chips, heads, vec_rows, main_ro...]
where the time goes in v3:
time: 112 us; the launch traced here: 111 us
  Pallas kernels  107 us (96%)
  local copies, waits for them, and re-layouts  4.22 us (4%)
    pallas_call x1, Pallas kernels, on_device(): pl.pallas_call(functools.partial(kernel, (chips, heads, vec_rows, main_ro...  107 us
    unnamed x5, local copies, waits for them, and re-layouts  4.22 us

profile of v3, /device:TPU:37, one launch (start us, length us, event | category | flops | bytes accessed | tf_op | source)
XLA Modules:
  0.0 111.4 jit_solution(11116676670208611078)
XLA Ops:
  0.6 106.5 %step.1 = (bf16[32,64]{1,0:T(8,128)(2,1)}, bf16[1,3,2560]{2,1,0:T(4,128)(2,1)}, f32[16,128,128]{2,1,0:T(8,128)}) custom-call(bf16[32,64]{1,0:T(8,128)(2,1)} %bitcast.16, bf16[1,3,2560]{2,1,0:T(4,128)(2,1)} %refs_1_.1, f32[16,128,128]{2,1,0:T(8,128)} %bitcast.13, bf16[32,2048]{1,0:T(8,128)(2,1)} %refs_3_.1, bf16[32,2048]{1,0:T(8,128)(2,1)} %refs_4_.1, ...), custom_call_target="tpu_custom_call" | custom-call | tf_op jit(solution)/shard_map/step/pallas_call | solution.py:660
  107.2 0.0 copy-start
  107.2 1.3 %copy.30 = bf16[64,32]{0,1:T(8,128)(2,1)} copy(bf16[64,32]{0,1:T(8,128)(2,1)} %bitcast.19) | data formatting | bytes 8192
  108.5 0.0 copy-done
  108.5 0.6 copy.31
  109.1 2.3 %copy.32 = f32[1,32,64,128]{3,2,1,0:T(8,128)} copy(f32[1,32,64,128]{3,2,1,0:T(8,128)} %bitcast.14) | data formatting | bytes 2097152
Async XLA Ops:
  107.2 1.3 %copy-start = (bf16[1,3,2560]{2,1,0:T(4,128)(2,1)S(1)}, bf16[1,3,2560]{2,1,0:T(4,128)(2,1)}, u32[]{:S(2)}) copy-start(bf16[1,3,2560]{2,1,0:T(4,128)(2,1)} %get-tuple-element.13) | copy-start | bytes 46084

commit v4 on v2

--- a/solution.py
+++ b/solution.py
@@ -10,7 +10,8 @@
 GROUPS = 2
 CAP = 8
 LANES = 128
-WINDOW = 8
+WINDOW = 16
+PIECES = 8
 RESIDUAL_SCALE = 2.0**0.25
 NORM_EPSILON = 1e-05
 GATED_EPSILON = 1e-06
@@ -54,7 +55,7 @@
         conv_rows, tap_rows, base_rows, chosen_s, spread_s,
         q_main, sa_main, ra_main, qb_main, sb_main, rb_main, sc_main, rc_main,
         q_gate, sa_gate, ra_gate, qb_gate, sb_gate, rb_gate, sc_gate, rc_gate,
-        fresh_row, n_rows, n_wide, r_rows, res_s, first_s, s_exp, r_exp, base_two, m_part, r_part, stat_s, final_s,
+        fresh_row, n_rows, n_wide, r_rows, res_s, first_s, s_exp, r_exp, base_two, m_part, r_part, stat_s, final_s, conv_s, result_s,
         local_sem, sib_sem, ssib_sem, round_sem, p_send, p_recv, x_send, x_recv, out_sem,
     ) = refs
     me = lax.axis_index("ep")
@@ -289,14 +290,16 @@
         return jnp.where(low, first, second)
 
     turned = jnp.concatenate(
-        [head_in * by_channel(step), by_channel(kept), jnp.zeros((LANES - 2 * vec_rows, LANES), F32)], axis=0
+        [head_in * by_channel(step), jnp.zeros((LANES - vec_rows, LANES), F32)], axis=0
     ).T
+    top = iota((LANES, LANES), 0) < LANES // 2
     lane = iota((LANES, LANES), 1)
     readout = jnp.zeros((LANES, LANES), F32)
     per_group = vec_rows // GROUPS
     for r in range(vec_rows):
         g = vec_rows + r // per_group
-        new = turned[:, vec_rows + r : vec_rows + r + 1] * x_state[r] + turned[:, r : r + 1] * active[g : g + 1]
+        keep = jnp.where(top, kept[:, 2 * r : 2 * r + 1], kept[:, 2 * r + 1 : 2 * r + 2])
+        new = keep * x_state[r] + turned[:, r : r + 1] * active[g : g + 1]
         x_state[r] = new
         seen = jnp.sum(new * active[g + GROUPS : g + GROUPS + 1], axis=1, keepdims=True)
         readout = jnp.where(lane == r, seen, readout)
@@ -334,7 +337,9 @@
     fresh_row[0 : taps - 2, :] = cache[1 : taps - 1]
     for k in range(conv_chunks):
         fresh_row[taps - 2 : taps - 1, k * LANES : (k + 1) * LANES] = fresh[k : k + 1]
-    o_conv[0] = fresh_row[...].astype(BF16)
+    conv_s[0] = fresh_row[...].astype(BF16)
+    conv_out = pltpu.make_async_copy(conv_s, o_conv, out_sem.at[1])
+    conv_out.start()
     own_tokens = one_hot(iota((chips, count), 1) == 2 * iota((chips, count), 0) + c)
     stream_cols = mm_nt(own_tokens, both)
     loads[6].wait()
@@ -430,20 +435,18 @@
         jnp.where(lane == 1, jnp.sum(square, axis=1, keepdims=True), 0.0),
     )
     pad = jnp.zeros((LANES - chips, LANES), F32)
-    stat_s[klass] = jnp.concatenate([sums, pad], axis=0).T[0:2]
-    for d in (x for k in range(WINDOW // 2, 0, -1) for x in (k, -k) if x != -(WINDOW // 2)):
-        send(stat_s.at[klass], stat_s.at[klass], x_send.at[5], x_recv.at[5], wrap(z + d, chips), c).start()
-    arrived(stat_s.at[pl.ds(0, WINDOW - 1)], x_recv.at[5])
-    sums = functools.reduce(lambda a, b: a + b, [stat_s[k] for k in range(WINDOW)])
-    sums = jnp.concatenate([sums, jnp.zeros((LANES - 2, LANES), F32)], axis=0).T
-    mean = sums[0:chips, 0:1] / width
-    variance = sums[0:chips, 1:2] / width - mean * mean
+    stat_s[c, klass] = jnp.concatenate([sums, pad], axis=0).T[0:2]
+    own_stat = stat_s.at[c, klass]
+    near = [x for k in range(WINDOW // 2, 0, -1) for x in (k, -k) if x != -(WINDOW // 2)]
+    for d in near:
+        for core in range(2):
+            send(own_stat, own_stat, x_send.at[5], x_recv.at[5], wrap(z + d, chips), core).start()
+    send(own_stat, own_stat, x_send.at[5], x_recv.at[5], z, 1 - c).start()
     block = z // WINDOW
     own = second[0]
     for j in range(1, tiles):
         own = jnp.where(block // 2 == j, second[j], own)
-    own = jnp.where(lax.rem(block, 2) == 0, own, half_turn(own))
-    final_s[c] = (own - mean) * lax.rsqrt(variance + NORM_EPSILON)
+    final_s[c] = jnp.where(lax.rem(block, 2) == 0, own, half_turn(own))
     swap_three = send(final_s.at[c], final_s.at[c], x_send.at[6], x_recv.at[6], z, 1 - c)
     swap_three.start()
     cols = x_sgain.shape[1]
@@ -454,8 +457,20 @@
     swap_three.wait_recv()
     full = final_s[...].reshape(count, LANES)
     full = jnp.where(c == 0, full, pltpu.roll(full, LANES - cols, 1))
+    stat_wait = stat_s.reshape(2 * WINDOW, 2, LANES).at[pl.ds(0, 2 * WINDOW - 1)]
+    arrived(stat_wait, x_recv.at[5])
+    mean, variance = [], []
+    for core in range(2):
+        sums = functools.reduce(lambda a, b: a + b, [stat_s[core, k] for k in range(WINDOW)])
+        sums = jnp.concatenate([sums, jnp.zeros((LANES - 2, LANES), F32)], axis=0).T
+        mean.append(sums[0:chips, 0:1] / width)
+        variance.append(sums[0:chips, 1:2] / width - mean[core] * mean[core])
+    mean, variance = jnp.concatenate(mean, axis=0), jnp.concatenate(variance, axis=0)
+    full = (full - mean) * lax.rsqrt(variance + NORM_EPSILON)
     full = (full * gain).astype(BF16)
-    o_result[...] = mm(mm_nt(take, full).astype(BF16), back).astype(BF16)
+    result_s[...] = mm(mm_nt(take, full).astype(BF16), back).astype(BF16)
+    result_out = pltpu.make_async_copy(result_s, o_result, out_sem.at[2])
+    result_out.start()
 
     for copy in swaps + [swap, swap_two, swap_three]:
         copy.wait_send()
@@ -463,8 +478,26 @@
         arrived(buffer, p_send.at[i])
     for i, buffer in ((0, n_rows), (1, r_rows), (3, r_exp)):
         arrived(buffer.at[pl.ds(0, chips - 1)], x_send.at[i])
-    arrived(stat_s.at[pl.ds(0, WINDOW - 1)], x_send.at[5])
+    arrived(stat_wait, x_send.at[5])
+    conv_out.wait()
     state_out.wait()
+    result_out.wait()
+
+
+def hand_out(result, conv, state, o_result, o_conv, o_state, x_result, x_conv, x_state, in_sem, out_sem):
+    moves = [(result, x_result, o_result), (conv, x_conv, o_conv)]
+    size = state.shape[0] // PIECES
+    for k in range(PIECES):
+        moves.append(tuple(ref.at[pl.ds(k * size, size)] for ref in (state, x_state, o_state)))
+    ins = [pltpu.make_async_copy(src, via, in_sem.at[i]) for i, (src, via, _) in enumerate(moves)]
+    outs = [pltpu.make_async_copy(via, dst, out_sem.at[i]) for i, (_, via, dst) in enumerate(moves)]
+    for copy in ins:
+        copy.start()
+    for first, second in zip(ins, outs):
+        first.wait()
+        second.start()
+    for copy in outs:
+        copy.wait()
 
 
 def on_device(
@@ -574,8 +607,10 @@
             pltpu.VMEM((tiles, chips, LANES), F32),
             pltpu.VMEM((2, tiles, chips, LANES), F32),
             pltpu.VMEM((tiles, chips, LANES), F32),
-            pltpu.VMEM((WINDOW, 2, LANES), F32),
+            pltpu.VMEM((2, WINDOW, 2, LANES), F32),
             pltpu.VMEM((2, chips, LANES), F32),
+            pltpu.VMEM(conv_cache.shape, BF16),
+            pltpu.VMEM((feats, tokens), BF16),
             pltpu.SemaphoreType.DMA((len(operands) - 1 + chunks,)),
             pltpu.SemaphoreType.DMA((len(doubled),)),
             pltpu.SemaphoreType.DMA((len(doubled),)),
@@ -584,10 +619,10 @@
             pltpu.SemaphoreType.DMA((6,)),
             pltpu.SemaphoreType.DMA((7,)),
             pltpu.SemaphoreType.DMA((7,)),
-            pltpu.SemaphoreType.DMA((1,)),
+            pltpu.SemaphoreType.DMA((3,)),
         ]
     )
-    result, new_conv, new_state = pl.pallas_call(
+    outs = pl.pallas_call(
         functools.partial(kernel, (chips, heads, vec_rows, main_rows, gate_rows)),
         out_shape=(
             jax.ShapeDtypeStruct((feats, tokens), BF16),
@@ -595,15 +630,21 @@
             jax.ShapeDtypeStruct(operands[2].shape, F32),
         ),
         in_specs=[pl.BlockSpec(memory_space=pltpu.HBM)] * len(operands),
-        out_specs=(
-            pl.BlockSpec(memory_space=pltpu.VMEM),
-            pl.BlockSpec(memory_space=pltpu.VMEM),
-            pl.BlockSpec(memory_space=pltpu.HBM),
-        ),
+        out_specs=(pl.BlockSpec(memory_space=pltpu.HBM),) * 3,
         scratch_shapes=scratch,
         compiler_params=pltpu.CompilerParams(collective_id=0, has_side_effects=True, vmem_limit_bytes=67043328),
         name="step",
     )(*operands)
+    result, new_conv, new_state = pl.pallas_call(
+        hand_out,
+        out_shape=tuple(jax.ShapeDtypeStruct(a.shape, a.dtype) for a in outs),
+        in_specs=[pl.BlockSpec(memory_space=pltpu.HBM)] * 3,
+        out_specs=(pl.BlockSpec(memory_space=pltpu.HBM),) * 3,
+        scratch_shapes=[pltpu.VMEM(a.shape, a.dtype) for a in outs]
+        + [pltpu.SemaphoreType.DMA((2 + PIECES,))] * 2,
+        compiler_params=pltpu.CompilerParams(vmem_limit_bytes=67043328),
+        name="hand_out",
+    )(*outs)
     return result.T, new_conv, new_state.reshape(scan_state.shape)
 
 

time: 107 us -> 101 us (0.944)
  local copies, waits for them, and re-layouts: 4.22 us -> 0 us
  Pallas kernels: 102 us -> 99.8 us
    unnamed x5 -> x0, local copies, waits for them, and re-layouts: 4.22 us -> none
    pallas_call x1, Pallas kernels: 102 us -> 97.7 us  [on_device(): pl.pallas_call(functools.partial(kernel, (chips, heads, vec_rows, main_ro...]
    pallas_call x0 -> x1, Pallas kernels: none -> 2.15 us  [on_device(): pl.pallas_call(hand_out, out_shape=tuple((jax.ShapeDtypeStruct(a.shape, a...]
where the time goes in v4:
time: 101 us; the launch traced here: 100 us
  Pallas kernels  99.8 us (99%)
    pallas_call x1, Pallas kernels, on_device(): pl.pallas_call(functools.partial(kernel, (chips, heads, vec_rows, main_ro...  97.7 us
    pallas_call x1, Pallas kernels, on_device(): pl.pallas_call(hand_out, out_shape=tuple((jax.ShapeDtypeStruct(a.shape, a...  2.15 us

profile of v4, /device:TPU:37, one launch (start us, length us, event | category | flops | bytes accessed | tf_op | source)
XLA Modules:
  0.0 100.5 jit_solution(1230880605454278478)
XLA Ops:
  0.6 97.7 %step.1 = (bf16[32,64]{1,0:T(8,128)(2,1)}, bf16[1,3,2560]{2,1,0:T(4,128)(2,1)}, f32[16,128,128]{2,1,0:T(8,128)}) custom-call(bf16[32,64]{1,0:T(8,128)(2,1)} %bitcast.15, bf16[1,3,2560]{2,1,0:T(4,128)(2,1)} %refs_1_.1, f32[16,128,128]{2,1,0:T(8,128)} %bitcast.13, bf16[32,2048]{1,0:T(8,128)(2,1)} %refs_3_.1, bf16[32,2048]{1,0:T(8,128)(2,1)} %refs_4_.1, ...), custom_call_target="tpu_custom_call" | custom-call | tf_op jit(solution)/shard_map/step/pallas_call | solution.py:625
  98.3 2.1 %hand_out.1 = (bf16[32,64]{1,0:T(8,128)(2,1)}, bf16[1,3,2560]{2,1,0:T(4,128)(2,1)}, f32[16,128,128]{2,1,0:T(8,128)}) custom-call(bf16[32,64]{1,0:T(8,128)(2,1)} %get-tuple-element.9.result, bf16[1,3,2560]{2,1,0:T(4,128)(2,1)} %get-tuple-element.10.conv, f32[16,128,128]{2,1,0:T(8,128)} %get-tuple-element.11.state), custom_call_target="tpu_custom_call" | custom-call | tf_op jit(solution)/shard_map/hand_out/pallas_call | solution.py:638

commit v5 on v4

--- a/solution.py
+++ b/solution.py
@@ -55,12 +55,13 @@
         conv_rows, tap_rows, base_rows, chosen_s, spread_s,
         q_main, sa_main, ra_main, qb_main, sb_main, rb_main, sc_main, rc_main,
         q_gate, sa_gate, ra_gate, qb_gate, sb_gate, rb_gate, sc_gate, rc_gate,
-        fresh_row, n_rows, n_wide, r_rows, res_s, first_s, s_exp, r_exp, base_two, m_part, r_part, stat_s, final_s, conv_s, result_s,
+        fresh_row, n_own, n_rows, n_wide, r_rows, res_s, first_s, s_exp, r_exp, base_two, m_part, r_part, stat_s, final_s, conv_s, result_s,
         local_sem, sib_sem, ssib_sem, round_sem, p_send, p_recv, x_send, x_recv, out_sem,
     ) = refs
     me = lax.axis_index("ep")
     z, c = me // 2, lax.rem(me, 2)
     p, h = lax.rem(z, 2), z // 2
+    q = 1 - c
     half = chips // 2
     quarter = half // 4
     pairs = half // 2
@@ -313,12 +314,12 @@
         part = gated[g * per_group : (g + 1) * per_group]
         mean = jnp.sum(part * part, keepdims=True) / (per_group * LANES)
         scale.append(part * lax.rsqrt(mean + GATED_EPSILON))
-    n_rows[z] = (jnp.concatenate(scale, axis=0) * x_ggain[...]).astype(BF16)
-
-    def to_everyone(ref, i, source):
+    n_own[...] = (jnp.concatenate(scale, axis=0) * x_ggain[...]).astype(BF16)
+
+    def to_everyone(ref, i, source, core):
         def one(d):
             target = wrap(z + d, chips)
-            send(source(target), ref.at[z], x_send.at[i], x_recv.at[i], target, c).start()
+            send(source(target), ref.at[z], x_send.at[i], x_recv.at[i], target, core).start()
 
         one(half)
 
@@ -332,7 +333,8 @@
     def from_everyone(ref, i):
         arrived(ref.at[pl.ds(0, chips - 1)], x_recv.at[i])
 
-    to_everyone(n_rows, 0, lambda target: n_rows.at[z])
+    to_everyone(n_rows, 0, lambda target: n_own, q)
+    send(n_own, n_rows.at[z], x_send.at[0], x_recv.at[0], z, q).start()
 
     fresh_row[0 : taps - 2, :] = cache[1 : taps - 1]
     for k in range(conv_chunks):
@@ -340,12 +342,12 @@
     conv_s[0] = fresh_row[...].astype(BF16)
     conv_out = pltpu.make_async_copy(conv_s, o_conv, out_sem.at[1])
     conv_out.start()
-    own_tokens = one_hot(iota((chips, count), 1) == 2 * iota((chips, count), 0) + c)
+    own_tokens = one_hot(iota((chips, count), 1) == 2 * iota((chips, count), 0) + q)
     stream_cols = mm_nt(own_tokens, both)
     loads[6].wait()
     swaps[6].wait_recv()
 
-    from_everyone(n_rows, 0)
+    arrived(n_rows, x_recv.at[0])
     n_wide[...] = n_rows[...].astype(F32).reshape(chips * vec_rows, LANES)
     normed = jnp.concatenate(
         [n_wide[pl.ds(k, chips, stride=vec_rows), :] for k in range(vec_rows)], axis=1
@@ -353,7 +355,7 @@
     mixed = mm_nt(normed, two(x_out)).astype(BF16).astype(F32)
     residual = RESIDUAL_SCALE * stream_cols + mixed
     r_rows[z] = jnp.concatenate([residual[: chips // 2], residual[chips // 2 :]], axis=1).astype(BF16)
-    to_everyone(r_rows, 1, lambda target: r_rows.at[z])
+    to_everyone(r_rows, 1, lambda target: r_rows.at[z], c)
     for i in range(18, len(loads)):
         loads[i].wait()
     from_everyone(r_rows, 1)
@@ -374,10 +376,10 @@
     mean = jnp.sum(total, axis=1, keepdims=True) / width
     scale = lax.rsqrt(jnp.sum(square, axis=1, keepdims=True) / width - mean * mean + NORM_EPSILON)
     for a in range(chunks):
-        first_s[c, a] = ((res_s[a] - mean) * scale * x_fgain[a : a + 1]).astype(BF16)
-    swap = send(first_s.at[c], first_s.at[c], x_send.at[2], x_recv.at[2], z, 1 - c)
+        first_s[q, a] = ((res_s[a] - mean) * scale * x_fgain[a : a + 1]).astype(BF16)
+    swap = send(first_s.at[q], first_s.at[q], x_send.at[2], x_recv.at[2], z, 1 - c)
     swap.start()
-    own_first = jnp.concatenate([first_s[c, a] for a in range(chunks)], axis=1)
+    own_first = jnp.concatenate([first_s[q, a] for a in range(chunks)], axis=1)
     shared = (silu(mm(own_first, x_sg[...])) * mm(own_first, x_su[...])).astype(BF16)
     swap.wait_recv()
 
@@ -401,7 +403,7 @@
             other = at + per_tile * LANES
             s_exp[r, j] = joined(out[:, at : at + LANES], out[:, other : other + LANES], r % 2).astype(BF16)
     klass = lax.rem(z, WINDOW)
-    to_everyone(r_exp, 3, lambda target: s_exp.at[lax.rem(target, WINDOW)])
+    to_everyone(r_exp, 3, lambda target: s_exp.at[lax.rem(target, WINDOW)], c)
     r_exp[z] = s_exp[klass]
 
     low = iota((chips, LANES), 1) < LANES // 2
@@ -411,7 +413,7 @@
         for i in (2 * j, 2 * j + 1):
             chunk = klass // 2 + per_tile * i
             part = mm(shared, x_sd[chunk]).astype(BF16).astype(F32)
-            sides.append(part + RESIDUAL_SCALE * first_s[c, chunk].astype(F32))
+            sides.append(part + RESIDUAL_SCALE * first_s[q, chunk].astype(F32))
         base_two[j] = jnp.where(p == 0, joined(*sides, 0), joined(*sides, 1))
 
     from_everyone(r_exp, 3)
@@ -421,10 +423,10 @@
         part = part[:count] + part[count:]
         for side in range(2):
             m_part[side, j] = part[side * chips : (side + 1) * chips]
-    swap_two = send(m_part.at[1 - c], r_part, x_send.at[4], x_recv.at[4], z, 1 - c)
+    swap_two = send(m_part.at[1 - q], r_part, x_send.at[4], x_recv.at[4], z, 1 - c)
     swap_two.start()
     swap_two.wait_recv()
-    second = [base_two[j] + m_part[c, j] + r_part[j] for j in range(tiles)]
+    second = [base_two[j] + m_part[q, j] + r_part[j] for j in range(tiles)]
 
     total = functools.reduce(lambda a, b: a + b, second)
     square = functools.reduce(lambda a, b: a + b, [s * s for s in second])
@@ -435,8 +437,8 @@
         jnp.where(lane == 1, jnp.sum(square, axis=1, keepdims=True), 0.0),
     )
     pad = jnp.zeros((LANES - chips, LANES), F32)
-    stat_s[c, klass] = jnp.concatenate([sums, pad], axis=0).T[0:2]
-    own_stat = stat_s.at[c, klass]
+    stat_s[q, klass] = jnp.concatenate([sums, pad], axis=0).T[0:2]
+    own_stat = stat_s.at[q, klass]
     near = [x for k in range(WINDOW // 2, 0, -1) for x in (k, -k) if x != -(WINDOW // 2)]
     for d in near:
         for core in range(2):
@@ -446,8 +448,8 @@
     own = second[0]
     for j in range(1, tiles):
         own = jnp.where(block // 2 == j, second[j], own)
-    final_s[c] = jnp.where(lax.rem(block, 2) == 0, own, half_turn(own))
-    swap_three = send(final_s.at[c], final_s.at[c], x_send.at[6], x_recv.at[6], z, 1 - c)
+    final_s[q] = jnp.where(lax.rem(block, 2) == 0, own, half_turn(own))
+    swap_three = send(final_s.at[q], final_s.at[q], x_send.at[6], x_recv.at[6], z, 1 - c)
     swap_three.start()
     cols = x_sgain.shape[1]
     gain = jnp.concatenate([x_sgain[...], jnp.zeros((1, LANES - cols), F32)], axis=1)
@@ -476,7 +478,8 @@
         copy.wait_send()
     for i, buffer in enumerate((sa_main, sa_gate, rb_main, rb_gate, rc_main, rc_gate)):
         arrived(buffer, p_send.at[i])
-    for i, buffer in ((0, n_rows), (1, r_rows), (3, r_exp)):
+    arrived(n_rows, x_send.at[0])
+    for i, buffer in ((1, r_rows), (3, r_exp)):
         arrived(buffer.at[pl.ds(0, chips - 1)], x_send.at[i])
     arrived(stat_wait, x_send.at[5])
     conv_out.wait()
@@ -597,6 +600,7 @@
         + projection(gate_rows)
         + [
             pltpu.VMEM((taps - 1, conv_weight.shape[1]), F32),
+            pltpu.VMEM((vec_rows, LANES), BF16),
             pltpu.VMEM((chips, vec_rows, LANES), BF16),
             pltpu.VMEM((chips * vec_rows, LANES), F32),
             pltpu.VMEM((chips, chips // 2, LANES), BF16),

time: 101 us -> 102 us (level)
  Pallas kernels: 99.8 us -> 101 us
    pallas_call x1, Pallas kernels: 97.7 us -> 99.1 us  [on_device(): pl.pallas_call(functools.partial(kernel, (chips, heads, vec_rows, main_ro...]
where the time goes in v5:
time: 102 us
  Pallas kernels  101 us (99%)
    pallas_call x1, Pallas kernels, on_device(): pl.pallas_call(functools.partial(kernel, (chips, heads, vec_rows, main_ro...  99.1 us
    pallas_call x1, Pallas kernels, on_device(): pl.pallas_call(hand_out, out_shape=tuple((jax.ShapeDtypeStruct(a.shape, a...  2.15 us

profile of v5, /device:TPU:37, one launch (start us, length us, event | category | flops | bytes accessed | tf_op | source)
XLA Modules:
  0.0 101.9 jit_solution(715950125864426063)
XLA Ops:
  0.6 99.1 %step.1 = (bf16[32,64]{1,0:T(8,128)(2,1)}, bf16[1,3,2560]{2,1,0:T(4,128)(2,1)}, f32[16,128,128]{2,1,0:T(8,128)}) custom-call(bf16[32,64]{1,0:T(8,128)(2,1)} %bitcast.15, bf16[1,3,2560]{2,1,0:T(4,128)(2,1)} %refs_1_.1, f32[16,128,128]{2,1,0:T(8,128)} %bitcast.13, bf16[32,2048]{1,0:T(8,128)(2,1)} %refs_3_.1, bf16[32,2048]{1,0:T(8,128)(2,1)} %refs_4_.1, ...), custom_call_target="tpu_custom_call" | custom-call | tf_op jit(solution)/shard_map/step/pallas_call | solution.py:629
  99.7 2.1 %hand_out.1 = (bf16[32,64]{1,0:T(8,128)(2,1)}, bf16[1,3,2560]{2,1,0:T(4,128)(2,1)}, f32[16,128,128]{2,1,0:T(8,128)}) custom-call(bf16[32,64]{1,0:T(8,128)(2,1)} %get-tuple-element.9.result, bf16[1,3,2560]{2,1,0:T(4,128)(2,1)} %get-tuple-element.10.conv, f32[16,128,128]{2,1,0:T(8,128)} %get-tuple-element.11.state), custom_call_target="tpu_custom_call" | custom-call | tf_op jit(solution)/shard_map/hand_out/pallas_call | solution.py:642

commit v6 on v5

--- a/solution.py
+++ b/solution.py
@@ -11,7 +11,7 @@
 CAP = 8
 LANES = 128
 WINDOW = 16
-PIECES = 8
+PIECES = 4
 RESIDUAL_SCALE = 2.0**0.25
 NORM_EPSILON = 1e-05
 GATED_EPSILON = 1e-06
@@ -56,7 +56,7 @@
         q_main, sa_main, ra_main, qb_main, sb_main, rb_main, sc_main, rc_main,
         q_gate, sa_gate, ra_gate, qb_gate, sb_gate, rb_gate, sc_gate, rc_gate,
         fresh_row, n_own, n_rows, n_wide, r_rows, res_s, first_s, s_exp, r_exp, base_two, m_part, r_part, stat_s, final_s, conv_s, result_s,
-        local_sem, sib_sem, ssib_sem, round_sem, p_send, p_recv, x_send, x_recv, out_sem,
+        local_sem, sib_sem, ssib_sem, round_sem, p_send, p_recv, x_send, x_recv, relay_sem, out_sem,
     ) = refs
     me = lax.axis_index("ep")
     z, c = me // 2, lax.rem(me, 2)
@@ -290,20 +290,43 @@
         second = jnp.sum(jnp.where(lane == 2 * at + 1, rows, 0.0), axis=1, keepdims=True)
         return jnp.where(low, first, second)
 
-    turned = jnp.concatenate(
-        [head_in * by_channel(step), jnp.zeros((LANES - vec_rows, LANES), F32)], axis=0
-    ).T
+    def parts(x):
+        high = x.astype(BF16).astype(F32)
+        return high, x - high
+
+    in_high, in_low = parts(head_in * by_channel(step))
+    vectors = active[vec_rows : vec_rows + 2 * GROUPS]
+    vec_high, vec_low = parts(vectors)
+    depth = 3 * vec_rows
+    stack = [in_high, in_low, in_high, vec_high, vec_low]
+    used = depth + 4 * GROUPS
+    turned = jnp.concatenate(stack + [jnp.zeros((LANES - used, LANES), F32)], axis=0).T
+    inputs = turned[:, 0:depth].astype(BF16)
     top = iota((LANES, LANES), 0) < LANES // 2
     lane = iota((LANES, LANES), 1)
+    at = iota((depth, LANES), 0)
     readout = jnp.zeros((LANES, LANES), F32)
     per_group = vec_rows // GROUPS
-    for r in range(vec_rows):
-        g = vec_rows + r // per_group
-        keep = jnp.where(top, kept[:, 2 * r : 2 * r + 1], kept[:, 2 * r + 1 : 2 * r + 2])
-        new = keep * x_state[r] + turned[:, r : r + 1] * active[g : g + 1]
-        x_state[r] = new
-        seen = jnp.sum(new * active[g + GROUPS : g + GROUPS + 1], axis=1, keepdims=True)
-        readout = jnp.where(lane == r, seen, readout)
+    readers = []
+    for g in range(GROUPS):
+        column = depth + GROUPS + g
+        both_parts = jnp.concatenate(
+            [jnp.broadcast_to(turned[:, k : k + 1], (LANES, LANES)) for k in (column, column + 2 * GROUPS)], axis=1
+        ).astype(BF16)
+        readers.append(jnp.concatenate([both_parts, both_parts], axis=0))
+    for r in range(0, vec_rows, 2):
+        g = r // per_group
+        entries = []
+        for n in (r, r + 1):
+            tail = jnp.where(at == n + 2 * vec_rows, vec_low[g : g + 1], 0.0)
+            entries.append(jnp.where((at == n) | (at == n + vec_rows), vec_high[g : g + 1], tail))
+        outer = mm(inputs, jnp.concatenate(entries, axis=1).astype(BF16))
+        for n in (r, r + 1):
+            keep = jnp.where(top, kept[:, 2 * n : 2 * n + 1], kept[:, 2 * n + 1 : 2 * n + 2])
+            new = keep * x_state[n] + outer[:, (n - r) * LANES : (n - r + 1) * LANES]
+            x_state[n] = new
+            seen = mm(jnp.concatenate(parts(new), axis=1).astype(BF16), readers[g])
+            readout = jnp.where(lane == n, seen[:, :LANES] + seen[:, LANES:], readout)
     state_out = pltpu.make_async_copy(x_state, o_state, out_sem.at[0])
     state_out.start()
     head_out = readout.T[0:vec_rows] + by_channel(x_skip[...]) * head_in
@@ -316,10 +339,10 @@
         scale.append(part * lax.rsqrt(mean + GATED_EPSILON))
     n_own[...] = (jnp.concatenate(scale, axis=0) * x_ggain[...]).astype(BF16)
 
-    def to_everyone(ref, i, source, core):
+    def to_everyone(ref, i, source):
         def one(d):
             target = wrap(z + d, chips)
-            send(source(target), ref.at[z], x_send.at[i], x_recv.at[i], target, core).start()
+            send(source(target), ref.at[z], x_send.at[i], x_recv.at[i], target, c).start()
 
         one(half)
 
@@ -333,7 +356,33 @@
     def from_everyone(ref, i):
         arrived(ref.at[pl.ds(0, chips - 1)], x_recv.at[i])
 
-    to_everyone(n_rows, 0, lambda target: n_own, q)
+    hop = chips // 8
+    relayed = half - 3
+    leaps = [(k, way) for k in range(hop, half, hop) for way in (1, -1)]
+
+    def spread_rows(i, row, ref, core):
+        def one(d, sem):
+            send(row, ref.at[z], x_send.at[i], sem, wrap(z + d, chips), core).start()
+
+        one(half, x_recv.at[i])
+        for k in range(half - 1, relayed, -1):
+            for way in (1, -1):
+                one(k * way, x_recv.at[i])
+        for n, (k, way) in reversed(list(enumerate(leaps))):
+            one(k * way, relay_sem.at[i, n])
+        for k in range(hop - 1, 0, -1):
+            for way in (1, -1):
+                one(k * way, x_recv.at[i])
+
+    def relay_rows(i, ref, count):
+        for n, (k, way) in enumerate(leaps):
+            source = wrap(z - k * way, chips)
+            arrived(ref.at[source], relay_sem.at[i, n])
+            for j in range(min(hop - 1, relayed - k), 0, -1):
+                send(ref.at[source], ref.at[source], x_send.at[i], x_recv.at[i], wrap(z + j * way, chips), c).start()
+        arrived(ref.at[pl.ds(0, count - len(leaps))], x_recv.at[i])
+
+    spread_rows(0, n_own, n_rows, q)
     send(n_own, n_rows.at[z], x_send.at[0], x_recv.at[0], z, q).start()
 
     fresh_row[0 : taps - 2, :] = cache[1 : taps - 1]
@@ -347,7 +396,7 @@
     loads[6].wait()
     swaps[6].wait_recv()
 
-    arrived(n_rows, x_recv.at[0])
+    relay_rows(0, n_rows, chips)
     n_wide[...] = n_rows[...].astype(F32).reshape(chips * vec_rows, LANES)
     normed = jnp.concatenate(
         [n_wide[pl.ds(k, chips, stride=vec_rows), :] for k in range(vec_rows)], axis=1
@@ -355,10 +404,10 @@
     mixed = mm_nt(normed, two(x_out)).astype(BF16).astype(F32)
     residual = RESIDUAL_SCALE * stream_cols + mixed
     r_rows[z] = jnp.concatenate([residual[: chips // 2], residual[chips // 2 :]], axis=1).astype(BF16)
-    to_everyone(r_rows, 1, lambda target: r_rows.at[z], c)
+    spread_rows(1, r_rows.at[z], r_rows, c)
     for i in range(18, len(loads)):
         loads[i].wait()
-    from_everyone(r_rows, 1)
+    relay_rows(1, r_rows, chips - 1)
 
     chunks = chips // 2
     low = iota((chips // 2, LANES), 1) < LANES // 2
@@ -403,7 +452,7 @@
             other = at + per_tile * LANES
             s_exp[r, j] = joined(out[:, at : at + LANES], out[:, other : other + LANES], r % 2).astype(BF16)
     klass = lax.rem(z, WINDOW)
-    to_everyone(r_exp, 3, lambda target: s_exp.at[lax.rem(target, WINDOW)], c)
+    to_everyone(r_exp, 3, lambda target: s_exp.at[lax.rem(target, WINDOW)])
     r_exp[z] = s_exp[klass]
 
     low = iota((chips, LANES), 1) < LANES // 2
@@ -623,6 +672,7 @@
             pltpu.SemaphoreType.DMA((6,)),
             pltpu.SemaphoreType.DMA((7,)),
             pltpu.SemaphoreType.DMA((7,)),
+            pltpu.SemaphoreType.DMA((2, 6)),
             pltpu.SemaphoreType.DMA((3,)),
         ]
     )

time: 102 us -> 98.8 us (0.969)
  Pallas kernels: 101 us -> 98 us
    pallas_call x1, Pallas kernels: 99.1 us -> 95.9 us  [on_device(): pl.pallas_call(functools.partial(kernel, (chips, heads, vec_rows, main_ro...]
where the time goes in v6:
time: 98.8 us; the launch traced here: 98.6 us
  Pallas kernels  98 us (99%)
    pallas_call x1, Pallas kernels, on_device(): pl.pallas_call(functools.partial(kernel, (chips, heads, vec_rows, main_ro...  95.9 us
    pallas_call x1, Pallas kernels, on_device(): pl.pallas_call(hand_out, out_shape=tuple((jax.ShapeDtypeStruct(a.shape, a...  2.05 us

profile of v6, /device:TPU:37, one launch (start us, length us, event | category | flops | bytes accessed | tf_op | source)
XLA Modules:
  0.0 98.6 jit_solution(11546480285248422385)
XLA Ops:
  0.6 95.9 %step.1 = (bf16[32,64]{1,0:T(8,128)(2,1)}, bf16[1,3,2560]{2,1,0:T(4,128)(2,1)}, f32[16,128,128]{2,1,0:T(8,128)}) custom-call(bf16[32,64]{1,0:T(8,128)(2,1)} %bitcast.15, bf16[1,3,2560]{2,1,0:T(4,128)(2,1)} %refs_1_.1, f32[16,128,128]{2,1,0:T(8,128)} %bitcast.13, bf16[32,2048]{1,0:T(8,128)(2,1)} %refs_3_.1, bf16[32,2048]{1,0:T(8,128)(2,1)} %refs_4_.1, ...), custom_call_target="tpu_custom_call" | custom-call | tf_op jit(solution)/shard_map/step/pallas_call | solution.py:679
  96.6 2.0 %hand_out.1 = (bf16[32,64]{1,0:T(8,128)(2,1)}, bf16[1,3,2560]{2,1,0:T(4,128)(2,1)}, f32[16,128,128]{2,1,0:T(8,128)}) custom-call(bf16[32,64]{1,0:T(8,128)(2,1)} %get-tuple-element.9.result, bf16[1,3,2560]{2,1,0:T(4,128)(2,1)} %get-tuple-element.10.conv, f32[16,128,128]{2,1,0:T(8,128)} %get-tuple-element.11.state), custom_call_target="tpu_custom_call" | custom-call | tf_op jit(solution)/shard_map/hand_out/pallas_call | solution.py:692

commit v7 on v6

--- a/solution.py
+++ b/solution.py
@@ -144,7 +144,7 @@
     slot = iota((CAP, count), 0).astype(F32)
     chosen_s[...] = one_hot((mine_member > 0.5) & (mine_rank == slot))
     wide = chips * CAP
-    pick = one_hot(iota((2 * chips, wide), 0) == 2 * (iota((2 * chips, wide), 1) // CAP) + c)
+    pick = one_hot(iota((2 * chips, wide), 0) == 2 * (iota((2 * chips, wide), 1) // CAP) + q)
     slot = lax.rem(iota((count, wide), 1), CAP).astype(F32)
     fits = (mm(member, pick) > 0.5) & (mm(rank, pick) == slot)
     spread_s[0:count, :] = jnp.where(fits, mm(w_hi, pick), 0.0).astype(BF16)
@@ -342,7 +342,7 @@
     def to_everyone(ref, i, source):
         def one(d):
             target = wrap(z + d, chips)
-            send(source(target), ref.at[z], x_send.at[i], x_recv.at[i], target, c).start()
+            send(source(target), ref.at[z], x_send.at[i], x_recv.at[i], target, q).start()
 
         one(half)
 
@@ -453,7 +453,7 @@
             s_exp[r, j] = joined(out[:, at : at + LANES], out[:, other : other + LANES], r % 2).astype(BF16)
     klass = lax.rem(z, WINDOW)
     to_everyone(r_exp, 3, lambda target: s_exp.at[lax.rem(target, WINDOW)])
-    r_exp[z] = s_exp[klass]
+    send(s_exp.at[klass], r_exp.at[z], x_send.at[3], x_recv.at[3], z, q).start()
 
     low = iota((chips, LANES), 1) < LANES // 2
     tiles = chunks // (2 * per_tile)
@@ -465,7 +465,7 @@
             sides.append(part + RESIDUAL_SCALE * first_s[q, chunk].astype(F32))
         base_two[j] = jnp.where(p == 0, joined(*sides, 0), joined(*sides, 1))
 
-    from_everyone(r_exp, 3)
+    arrived(r_exp, x_recv.at[3])
     for j in range(tiles):
         rows = r_exp[:, j].astype(F32).reshape(chips * CAP, LANES).astype(BF16)
         part = mm(spread_s[...], rows)
@@ -528,8 +528,8 @@
     for i, buffer in enumerate((sa_main, sa_gate, rb_main, rb_gate, rc_main, rc_gate)):
         arrived(buffer, p_send.at[i])
     arrived(n_rows, x_send.at[0])
-    for i, buffer in ((1, r_rows), (3, r_exp)):
-        arrived(buffer.at[pl.ds(0, chips - 1)], x_send.at[i])
+    arrived(r_rows.at[pl.ds(0, chips - 1)], x_send.at[1])
+    arrived(r_exp, x_send.at[3])
     arrived(stat_wait, x_send.at[5])
     conv_out.wait()
     state_out.wait()

time: 98.8 us -> 98.6 us (level)
  no operation moved by 1% of the time
where the time goes in v7:
time: 98.6 us; the launch traced here: 98.5 us
  Pallas kernels  97.8 us (99%)
    pallas_call x1, Pallas kernels, on_device(): pl.pallas_call(functools.partial(kernel, (chips, heads, vec_rows, main_ro...  95.8 us
    pallas_call x1, Pallas kernels, on_device(): pl.pallas_call(hand_out, out_shape=tuple((jax.ShapeDtypeStruct(a.shape, a...  2.05 us

profile of v7, /device:TPU:37, one launch (start us, length us, event | category | flops | bytes accessed | tf_op | source)
XLA Modules:
  0.0 98.5 jit_solution(3540355023423171556)
XLA Ops:
  0.6 95.8 %step.1 = (bf16[32,64]{1,0:T(8,128)(2,1)}, bf16[1,3,2560]{2,1,0:T(4,128)(2,1)}, f32[16,128,128]{2,1,0:T(8,128)}) custom-call(bf16[32,64]{1,0:T(8,128)(2,1)} %bitcast.15, bf16[1,3,2560]{2,1,0:T(4,128)(2,1)} %refs_1_.1, f32[16,128,128]{2,1,0:T(8,128)} %bitcast.13, bf16[32,2048]{1,0:T(8,128)(2,1)} %refs_3_.1, bf16[32,2048]{1,0:T(8,128)(2,1)} %refs_4_.1, ...), custom_call_target="tpu_custom_call" | custom-call | tf_op jit(solution)/shard_map/step/pallas_call | solution.py:679
  96.4 2.0 %hand_out.1 = (bf16[32,64]{1,0:T(8,128)(2,1)}, bf16[1,3,2560]{2,1,0:T(4,128)(2,1)}, f32[16,128,128]{2,1,0:T(8,128)}) custom-call(bf16[32,64]{1,0:T(8,128)(2,1)} %get-tuple-element.9.result, bf16[1,3,2560]{2,1,0:T(4,128)(2,1)} %get-tuple-element.10.conv, f32[16,128,128]{2,1,0:T(8,128)} %get-tuple-element.11.state), custom_call_target="tpu_custom_call" | custom-call | tf_op jit(solution)/shard_map/hand_out/pallas_call | solution.py:692
